TPU v7x, 32 devices: a whole 2x2x4 slice. The times are simulated.
32 devices in a mesh: grp: 2 (over x), ep: 16 (over z, y, core).
Axes of the slice: x: 2, y: 2, z: 4, core: 2. Of those that a mesh axis runs over, the one named last changes fastest.
Arguments:
- tokens: bfloat16 [16384, 2048], P(('grp', 'ep')), parts along dimension 0, may hold values from -6 to 6
- norm_gain: float32 [2048], replicated, may hold values from 0.1 to 1.9
- route_ids: int32 [16384, 2], P(('grp', 'ep')), parts along dimension 0, may hold values from 0 to 15, all different within a row; in each aligned block of 512 rows (0 to 511, 512 to 1023, ...) at most 96 rows name the same one
- route_gates: float32 [16384, 2], P(('grp', 'ep')), parts along dimension 0, may hold values from 0.05 to 1
- w_gate: bfloat16 [16, 2048, 1024], P('ep'), may hold values from -0.125 to 0.125
- w_up: bfloat16 [16, 2048, 1024], P('ep'), may hold values from -0.125 to 0.125
- w_down: bfloat16 [16, 1024, 2048], P('ep'), may hold values from -0.1875 to 0.1875
Outputs:
- mixed: bfloat16 [16384, 2048], P(('grp', 'ep')), parts along dimension 0
There are 2 independent parts, one for each index of `grp`. A program takes and returns all parts, laid end to end along the dimension named above; an argument that names none is the same for every part. Nothing has to cross between parts.
Inputs may be any that keep to these rules, and one draw needn't show every extreme that they name: `route_ids`: each row names 2 different experts. Among the rows of one device no expert is named more than 96 times, and in some devices' rows one expert is named exactly 96 times.
All inputs are finite; a program needn't handle non-finite values.
Results may differ from a plain program's by a relative error of at most 0.0071.
Values may be sent and summed in bfloat16 or wider, within the bound.
A program may use at most 128 MiB of HBM per device.

v0:
```python
import functools

import jax
import jax.numpy as jnp
from jax import lax
from jax.experimental import pallas as pl
from jax.experimental.pallas import tpu as pltpu
from jax.sharding import PartitionSpec as P

EPS = 1e-06
CHUNKS = 4
TILE = 256
VMEM_BYTES = 66000000


def slot_index(route_ids, experts, capacity):
    rows, top = route_ids.shape
    hit = [route_ids[:, k : k + 1] == jnp.arange(experts, dtype=jnp.int32)[None, :] for k in range(top)]
    named = sum(h.astype(jnp.float32) for h in hit)
    before = (jnp.arange(rows)[:, None] > jnp.arange(rows)[None, :]).astype(jnp.bfloat16)
    ranked = jnp.dot(before, named.astype(jnp.bfloat16), preferred_element_type=jnp.float32)
    base = ranked + jnp.arange(experts, dtype=jnp.float32)[None, :] * capacity
    return jnp.stack([jnp.sum(jnp.where(h, base, 0.0), axis=1) for h in hit])


def dot32(a, b):
    return jnp.dot(a, b, preferred_element_type=jnp.float32)


def kernel(
    devices, capacity, top,
    tokens_hbm, gain, table, gate_hbm, up_hbm, down_hbm,
    mixed,
    normed, far, far_table, takes, highs, lows, packed, arrived, hidden, w_gate, w_up, w_down,
    outs, backs, partial, partial_in,
    weight_sems, table_sems, far_send, far_recv, own_sems, self_sems, go_send, go_recv,
    back_send, back_recv, part_send, part_recv,
):
    half = devices // 2
    chunks, rows, step = normed.shape
    count = half * capacity
    ff = w_gate.shape[1]
    me = lax.axis_index("ep")
    q = me % half
    base = me - q
    partner = (me + half) % devices
    first = base * capacity

    def peer_at(i):
        off = (half // 2 + i) % half + (half // 2 + i) // half
        return (q + off) % half

    barrier = pltpu.get_barrier_semaphore()

    def greet(i, carry):
        pl.semaphore_signal(barrier, inc=1, device_id={"ep": base + peer_at(i)})
        return carry

    token_load = pltpu.make_async_copy(tokens_hbm, mixed, weight_sems.at[3])
    token_load.start()
    lax.fori_loop(0, half - 1, greet, 0)
    pl.semaphore_signal(barrier, inc=1, device_id={"ep": partner})

    loads = [
        pltpu.make_async_copy(gate_hbm.at[0], w_gate, weight_sems.at[0]),
        pltpu.make_async_copy(up_hbm.at[0], w_up, weight_sems.at[1]),
        pltpu.make_async_copy(down_hbm.at[0], w_down, weight_sems.at[2]),
    ]
    token_load.wait()

    def norm(i, carry):
        at = pl.ds(pl.multiple_of(i * 64, 64), 64)
        floats = mixed[at, :].astype(jnp.float32)
        scale = lax.rsqrt(jnp.mean(floats * floats, axis=-1, keepdims=True) + EPS)
        value = (floats * scale * gain[...]).astype(jnp.bfloat16)
        for c in range(chunks):
            normed[c, at, :] = value[:, c * step : (c + 1) * step]
        return carry

    lax.fori_loop(0, rows // 64, norm, 0)
    pl.semaphore_wait(barrier, half)

    def remote(src, dst, send, recv, device):
        return pltpu.make_async_remote_copy(
            src_ref=src, dst_ref=dst, send_sem=send, recv_sem=recv, device_id={"ep": device}
        )

    def table_copy():
        return remote(table, far_table, table_sems.at[0], table_sems.at[1], partner)

    def far_copy(c):
        return remote(normed.at[c], far.at[c], far_send.at[c], far_recv.at[c], partner)

    def part_copy(c):
        return remote(partial.at[c], partial_in.at[c], part_send.at[c], part_recv.at[c], partner)

    def span(j):
        return pl.ds(pl.multiple_of(j * capacity, 16), capacity)

    def go_copy(s, c, peer, slot):
        return remote(
            packed.at[s, c, span(peer)], arrived.at[s, c, span(q)],
            go_send.at[s, c, slot], go_recv.at[s, c, q], base + peer,
        )

    def back_copy(s, c, peer, slot):
        return remote(
            outs.at[s, c, span(peer)], backs.at[s, c, span(q)],
            back_send.at[s, c, slot], back_recv.at[s, c, q], base + peer,
        )

    def go_arrival(s, c, peer):
        return remote(
            packed.at[s, c, span(peer)], arrived.at[s, c, span(peer)],
            go_send.at[s, c, 0], go_recv.at[s, c, peer], base + peer,
        )

    def back_arrival(s, c, peer):
        return remote(
            outs.at[s, c, span(peer)], backs.at[s, c, span(peer)],
            back_send.at[s, c, 0], back_recv.at[s, c, peer], base + peer,
        )

    def go_self(s, c):
        return pltpu.make_async_copy(packed.at[s, c, span(q)], arrived.at[s, c, span(q)], own_sems.at[s, c])

    def back_self(s, c):
        return pltpu.make_async_copy(outs.at[s, c, span(q)], backs.at[s, c, span(q)], self_sems.at[s, c])

    def each_peer(act):
        def one(i, carry):
            act(peer_at(i), i)
            return carry

        lax.fori_loop(0, half - 1, one, 0)

    def matrices(s, source):
        width = 128

        def one(i, carry):
            at = pl.multiple_of(i * width, width)
            slots = (first + at + lax.broadcasted_iota(jnp.int32, (width, rows), 0)).astype(jnp.float32)
            taken = jnp.zeros((width, rows), jnp.float32)
            total = jnp.zeros((width, rows), jnp.float32)
            for k in range(top):
                hit = source[k : k + 1, :] == slots
                taken = taken + jnp.where(hit, 1.0, 0.0)
                total = total + jnp.where(hit, source[top + k : top + k + 1, :], 0.0)
            takes[s, pl.ds(at, width), :] = taken.astype(jnp.bfloat16)
            turned = total.T
            high = turned.astype(jnp.bfloat16)
            highs[s, :, pl.ds(at, width)] = high
            lows[s, :, pl.ds(at, width)] = (turned - high.astype(jnp.float32)).astype(jnp.bfloat16)
            return carry

        lax.fori_loop(0, count // width, one, 0)

    def tiles(act):
        def one(i, carry):
            act(pl.ds(pl.multiple_of(i * TILE, TILE), TILE))
            return carry

        lax.fori_loop(0, step // TILE, one, 0)

    def pack(s, c, source):
        def one(cols):
            packed[s, c, :, cols] = dot32(takes[s], source[c, :, cols]).astype(jnp.bfloat16)

        tiles(one)
        each_peer(lambda peer, i: go_copy(s, c, peer, i).start())
        go_self(s, c).start()

    def wait_go(s, c):
        each_peer(lambda peer, i: go_arrival(s, c, peer).wait_recv())
        go_self(s, c).wait()

    def expert_hidden(s):
        def one(i, carry):
            cols = pl.ds(pl.multiple_of(i * TILE, TILE), TILE)
            gate_pre = dot32(arrived[s, 0], w_gate[0:step, cols])
            up_pre = dot32(arrived[s, 0], w_up[0:step, cols])
            for c in range(1, chunks):
                gate_pre += dot32(arrived[s, c], w_gate[c * step : (c + 1) * step, cols])
                up_pre += dot32(arrived[s, c], w_up[c * step : (c + 1) * step, cols])
            hidden[s, :, cols] = (gate_pre / (1.0 + jnp.exp(-gate_pre)) * up_pre).astype(jnp.bfloat16)
            return carry

        lax.fori_loop(0, ff // TILE, one, 0)

    def expert_out(s, c):
        def one(i, carry):
            at = pl.multiple_of(i * TILE, TILE)
            cols = pl.ds(pl.multiple_of(c * step + at, TILE), TILE)
            outs[s, c, :, pl.ds(at, TILE)] = dot32(hidden[s], w_down[:, cols]).astype(jnp.bfloat16)
            return carry

        lax.fori_loop(0, step // TILE, one, 0)

    def send_back(s, c):
        each_peer(lambda peer, i: back_copy(s, c, peer, i).start())
        back_self(s, c).start()

    def wait_back(s, c):
        each_peer(lambda peer, i: back_arrival(s, c, peer).wait_recv())
        back_self(s, c).wait()

    table_copy().start()
    far_copy(0).start()
    for load in loads:
        load.start()
    matrices(0, table)
    for c in range(chunks):
        pack(0, c, normed)
        if c + 1 < chunks:
            far_copy(c + 1).start()
    table_copy().wait()
    matrices(1, far_table)
    for c in range(chunks):
        far_copy(c).wait_recv()
        pack(1, c, far)
        if c == chunks - 2:
            for s_c in range(chunks):
                wait_go(0, s_c)
            for load in loads:
                load.wait()
            expert_hidden(0)
            for d in range(chunks):
                expert_out(0, d)
    for c in range(chunks):
        wait_go(1, c)
    for c in range(1):
        send_back(0, c)
    expert_hidden(1)
    for c in range(chunks):
        expert_out(1, c)
        send_back(1, c)
    for c in range(chunks):
        wait_back(1, c)

        def merge(cols):
            back = backs[1, c, :, cols]
            partial[c, :, cols] = (dot32(highs[1], back) + dot32(lows[1], back)).astype(jnp.bfloat16)

        tiles(merge)
        part_copy(c).start()
        if c >= 1:
            send_back(0, c)
    for c in range(chunks):
        wait_back(0, c)
        part_copy(c).wait_recv()

        def close(i, carry):
            at = pl.multiple_of(i * TILE, TILE)
            cols = pl.ds(at, TILE)
            back = backs[0, c, :, cols]
            total = dot32(highs[0], back) + dot32(lows[0], back) + partial_in[c, :, cols].astype(jnp.float32)
            mixed[:, pl.ds(pl.multiple_of(c * step + at, TILE), TILE)] = total.astype(jnp.bfloat16)
            return carry

        lax.fori_loop(0, step // TILE, close, 0)
    for c in range(chunks):
        far_copy(c).wait_send()
        part_copy(c).wait_send()
        for s in range(2):
            each_peer(lambda peer, i: go_copy(s, c, peer, i).wait_send())
            each_peer(lambda peer, i: back_copy(s, c, peer, i).wait_send())


def body(tokens, norm_gain, route_ids, route_gates, w_gate, w_up, w_down):
    rows, width = tokens.shape
    top = route_ids.shape[1]
    devices = lax.axis_size("ep")
    experts = devices
    ff = w_gate.shape[2]
    capacity = 3 * rows * top // (2 * experts)
    half = devices // 2
    count = half * capacity
    step = width // CHUNKS
    weights = (route_gates / jnp.sum(route_gates, axis=1, keepdims=True)).T
    table = jnp.concatenate([slot_index(route_ids, experts, capacity), weights])
    vmem = pl.BlockSpec(memory_space=pltpu.VMEM)
    hbm = pl.BlockSpec(memory_space=pl.ANY)
    bf16 = jnp.bfloat16
    dma = pltpu.SemaphoreType.DMA
    return pl.pallas_call(
        functools.partial(kernel, devices, capacity, top),
        out_shape=jax.ShapeDtypeStruct((rows, width), bf16),
        in_specs=[hbm, vmem, vmem, hbm, hbm, hbm],
        out_specs=vmem,
        scratch_shapes=[
            pltpu.VMEM((CHUNKS, rows, step), bf16),
            pltpu.VMEM((CHUNKS, rows, step), bf16),
            pltpu.VMEM(table.shape, jnp.float32),
            pltpu.VMEM((2, count, rows), bf16),
            pltpu.VMEM((2, rows, count), bf16),
            pltpu.VMEM((2, rows, count), bf16),
            pltpu.VMEM((2, CHUNKS, count, step), bf16),
            pltpu.VMEM((2, CHUNKS, count, step), bf16),
            pltpu.VMEM((2, count, ff), bf16),
            pltpu.VMEM((width, ff), bf16),
            pltpu.VMEM((width, ff), bf16),
            pltpu.VMEM((ff, width), bf16),
            pltpu.VMEM((2, CHUNKS, count, step), bf16),
            pltpu.VMEM((2, CHUNKS, count, step), bf16),
            pltpu.VMEM((CHUNKS, rows, step), bf16),
            pltpu.VMEM((CHUNKS, rows, step), bf16),
            dma((4,)),
            dma((2,)),
            dma((CHUNKS,)),
            dma((CHUNKS,)),
            dma((2, CHUNKS)),
            dma((2, CHUNKS)),
            dma((2, CHUNKS, half)),
            dma((2, CHUNKS, half)),
            dma((2, CHUNKS, half)),
            dma((2, CHUNKS, half)),
            dma((CHUNKS,)),
            dma((CHUNKS,)),
        ],
        compiler_params=pltpu.CompilerParams(
            collective_id=0, has_side_effects=True, vmem_limit_bytes=VMEM_BYTES
        ),
    )(tokens, norm_gain[None, :], table, w_gate, w_up, w_down)


def solution(mesh):
    placed = (
        P(("grp", "ep"), None),
        P(),
        P(("grp", "ep"), None),
        P(("grp", "ep"), None),
        P("ep", None, None),
        P("ep", None, None),
        P("ep", None, None),
    )
    return jax.shard_map(
        body, mesh=mesh, in_specs=placed, out_specs=P(("grp", "ep"), None), check_vma=False
    )
```

profile of v0, /device:TPU:15, one launch (start us, length us, event | category | flops | bytes accessed | tf_op | source)
XLA Modules:
  0.0 245.5 jit_solution(16343209545891360338)
XLA Ops:
  0.0 0.7 reduce_sum.29
  0.7 0.7 divide_bitcast_fusion
  1.4 0.8 fusion.2
  2.2 0.3 select_reduce_fusion.1
  2.4 0.6 pad_maximum_fusion.table
  3.1 239.2 %shard_map.73 = bf16[512,2048]{1,0:T(8,128)(2,1)} custom-call(bf16[512,2048]{1,0:T(8,128)(2,1)} %tokens_hbm.1, f32[1,2048]{1,0:T(1,128)} %bitcast.7, f32[4,512]{1,0:T(4,128)} %pad_maximum_fusion.table, bf16[1,2048,1024]{2,1,0:T(8,128)(2,1)} %gate_hbm.1, bf16[1,2048,1024]{2,1,0:T(8,128)(2,1)} %up_hbm.1, bf16[1,1024,2048]{2,1,0:T(8,128)(2,1)} %down_hbm.1), custom_call_target="tpu_custom_call" | custom-call | tf_op jit(solution)/shard_map/pallas_call | solution.py:285
  242.3 3.2 %copy.9 = bf16[512,2048]{1,0:T(8,128)(2,1)} copy(bf16[512,2048]{1,0:T(8,128)(2,1)} %shard_map.73) | data formatting | bytes 4194304
  (1 shorter events, 0.0 us)
where the time goes:
time: 248 us; the launch traced here: 245 us
  Pallas kernels  239 us (96%)
  local copies, waits for them, and re-layouts  3.93 us (2%)
    pallas_call x1, Pallas kernels, body(): pl.pallas_call(functools.partial(kernel, devices, capacity, top), out_sha...  239 us

commit v1 on v0

v1 whole, which is shorter than its diff:
```python
import functools

import jax
import jax.numpy as jnp
from jax import lax
from jax.experimental import pallas as pl
from jax.experimental.pallas import tpu as pltpu
from jax.sharding import PartitionSpec as P

EPS = 1e-06
CHUNKS = 4
TILE = 256
VMEM_BYTES = 67000000


def slot_index(route_ids, experts, capacity):
    rows, top = route_ids.shape
    hit = [route_ids[:, k : k + 1] == jnp.arange(experts, dtype=jnp.int32)[None, :] for k in range(top)]
    named = sum(h.astype(jnp.float32) for h in hit)
    before = (jnp.arange(rows)[:, None] > jnp.arange(rows)[None, :]).astype(jnp.bfloat16)
    ranked = jnp.dot(before, named.astype(jnp.bfloat16), preferred_element_type=jnp.float32)
    base = ranked + jnp.arange(experts, dtype=jnp.float32)[None, :] * capacity
    return jnp.stack([jnp.sum(jnp.where(h, base, 0.0), axis=1) for h in hit])


def dot32(a, b):
    return jnp.dot(a, b, preferred_element_type=jnp.float32)


HOME, ACROSS, BEYOND, NEAR = range(4)


def kernel(
    devices, capacity, top,
    tokens_hbm, gain, table, gate_hbm, up_hbm, down_hbm,
    mixed,
    normed, far, tables, takes, gives, take_near, give_near, packed, packed_near, arrived, hidden,
    w_gate, w_up, w_down, backs, backs_near, partial_in,
    load_sems, table_send, table_recv, far_send, far_recv, go_send, go_recv, back_send, back_recv,
    relay_send, relay_recv, part_send, part_recv,
):
    m = devices // 4
    half = 2 * m
    unit = m * capacity
    chunks, rows, step = normed.shape
    ff = w_gate.shape[1]
    me = lax.axis_index("ep")
    side = me // half
    plane = me // m
    j = me % m
    q = me % half
    own = plane * m
    hub = (1 + side) * m
    leaf = 3 * side * m
    other_hub = (2 - side) * m + j
    is_hub = plane * (3 - plane) > 0

    barrier = pltpu.get_barrier_semaphore()

    def greet(i, carry):
        pl.semaphore_signal(barrier, inc=1, device_id={"ep": side * half + (q + 1 + i) % half})
        return carry

    token_load = pltpu.make_async_copy(tokens_hbm, mixed, load_sems.at[3])
    token_load.start()
    lax.fori_loop(0, half - 1, greet, 0)

    @pl.when(is_hub)
    def _():
        pl.semaphore_signal(barrier, inc=1, device_id={"ep": other_hub})

    loads = [
        pltpu.make_async_copy(gate_hbm.at[0], w_gate, load_sems.at[0]),
        pltpu.make_async_copy(up_hbm.at[0], w_up, load_sems.at[1]),
        pltpu.make_async_copy(down_hbm.at[0], w_down, load_sems.at[2]),
    ]
    token_load.wait()

    def norm(i, carry):
        at = pl.ds(pl.multiple_of(i * 64, 64), 64)
        floats = mixed[at, :].astype(jnp.float32)
        scale = lax.rsqrt(jnp.mean(floats * floats, axis=-1, keepdims=True) + EPS)
        value = (floats * scale * gain[...]).astype(jnp.bfloat16)
        for c in range(chunks):
            normed[c, at, :] = value[:, c * step : (c + 1) * step]
        return carry

    lax.fori_loop(0, rows // 64, norm, 0)

    @pl.when(is_hub)
    def _():
        pl.semaphore_wait(barrier, half)

    @pl.when(jnp.logical_not(is_hub))
    def _():
        pl.semaphore_wait(barrier, half - 1)

    def remote(src, dst, send, recv, device):
        return pltpu.make_async_remote_copy(
            src_ref=src, dst_ref=dst, send_sem=send, recv_sem=recv, device_id={"ep": device}
        )

    def table_copy(r, src, device):
        return remote(src, tables.at[r - 1], table_send.at[r - 1], table_recv.at[r - 1], device)

    def far_copy(r, c, src, device):
        return remote(src.at[c], far.at[r - 1, c], far_send.at[r - 1, c], far_recv.at[r - 1, c], device)

    def part_copy(k, c, src, slot, device):
        return remote(src.at[c], partial_in.at[slot, c], part_send.at[k, c], part_recv.at[slot, c], device)

    def span(i, part=0):
        return pl.ds(pl.multiple_of(part * unit + i * capacity, 16), capacity)

    def packs(r, c):
        return packed_near.at[c] if r == NEAR else packed.at[r, c]

    def returns(r, c):
        return backs_near.at[c] if r == NEAR else backs.at[r, c]

    def go_copy(r, c, part, i):
        target = (leaf if part else own) + i
        return remote(
            packs(r, c).at[span(i, part)], arrived.at[r, c, span(j)],
            go_send.at[r, c, part * m + i], go_recv.at[r, c, j], target,
        )

    def go_arrival(r, c, i, base):
        return remote(
            arrived.at[r, c, span(i)], arrived.at[r, c, span(i)],
            go_send.at[r, c, 0], go_recv.at[r, c, i], base + i,
        )

    def back_copy(r, c, i):
        return remote(
            arrived.at[r, c, span(i)], returns(r, c).at[span(j)],
            back_send.at[r, c, i], back_recv.at[r, c, j], own + i,
        )

    def back_arrival(r, c, i):
        return remote(
            arrived.at[r, c, span(i)], returns(r, c).at[span(i)],
            back_send.at[r, c, 0], back_recv.at[r, c, i], own + i,
        )

    def relay_copy(r, c):
        return remote(
            backs.at[r, c, pl.ds(0, unit)], backs.at[r, c, pl.ds(unit, unit)],
            relay_send.at[r, c], relay_recv.at[r, c], hub + j,
        )

    def others(act):
        def one(i, carry):
            act((j + 1 + i) % m)
            return carry

        lax.fori_loop(0, m - 1, one, 0)

    def everyone(act):
        def one(i, carry):
            act((j + i) % m)
            return carry

        lax.fori_loop(0, m, one, 0)

    def matrices(source, take, give, bases):
        width = 128

        def block(part, first):
            def one(i, carry):
                at = pl.multiple_of(part * unit + i * width, width)
                start = first * capacity + i * width
                slots = (start + lax.broadcasted_iota(jnp.int32, (width, rows), 0)).astype(jnp.float32)
                taken = jnp.zeros((width, rows), jnp.float32)
                total = jnp.zeros((width, rows), jnp.float32)
                for k in range(top):
                    hit = source[k : k + 1, :] == slots
                    taken = taken + jnp.where(hit, 1.0, 0.0)
                    total = total + jnp.where(hit, source[top + k : top + k + 1, :], 0.0)
                take[pl.ds(at, width), :] = taken.astype(jnp.bfloat16)
                give[:, pl.ds(at, width)] = total.T.astype(jnp.bfloat16)
                return carry

            lax.fori_loop(0, unit // width, one, 0)

        for part, first in enumerate(bases):
            block(part, first)

    def tiles(act):
        def one(i, carry):
            act(pl.ds(pl.multiple_of(i * TILE, TILE), TILE))
            return carry

        lax.fori_loop(0, step // TILE, one, 0)

    def pack(r, c, source):
        take = take_near if r == NEAR else takes.at[r]
        target = packs(r, c)

        def one(cols):
            target[:, cols] = dot32(take[...], source[c, :, cols]).astype(jnp.bfloat16)

        tiles(one)
        if r != NEAR:
            everyone(lambda i: go_copy(r, c, 1, i).start())
        others(lambda i: go_copy(r, c, 0, i).start())
        arrived[r, c, span(j), :] = target[span(j), :]

    def expert(r):
        def gated(i, carry):
            cols = pl.ds(pl.multiple_of(i * TILE, TILE), TILE)
            gate_pre = dot32(arrived[r, 0], w_gate[0:step, cols])
            up_pre = dot32(arrived[r, 0], w_up[0:step, cols])
            for c in range(1, chunks):
                gate_pre += dot32(arrived[r, c], w_gate[c * step : (c + 1) * step, cols])
                up_pre += dot32(arrived[r, c], w_up[c * step : (c + 1) * step, cols])
            hidden[:, cols] = (gate_pre / (1.0 + jnp.exp(-gate_pre)) * up_pre).astype(jnp.bfloat16)
            return carry

        lax.fori_loop(0, ff // TILE, gated, 0)
        for c in range(chunks):

            def out(i, carry):
                at = pl.multiple_of(i * TILE, TILE)
                cols = pl.ds(pl.multiple_of(c * step + at, TILE), TILE)
                arrived[r, c, :, pl.ds(at, TILE)] = dot32(hidden[...], w_down[:, cols]).astype(jnp.bfloat16)
                return carry

            lax.fori_loop(0, step // TILE, out, 0)
            others(lambda i: back_copy(r, c, i).start())
            returns(r, c)[span(j), :] = arrived[r, c, span(j), :]

    def wait_back(r, c):
        others(lambda i: back_arrival(r, c, i).wait_recv())

    def hub_role():
        bases = (hub, leaf)
        far_copy(ACROSS, 0, normed, other_hub).start()
        table_copy(ACROSS, table, other_hub).start()
        for load in loads:
            load.start()
        matrices(table, takes.at[HOME], gives.at[HOME], bases)
        table_copy(NEAR, table, leaf + j).wait_recv()
        table_copy(BEYOND, tables.at[NEAR - 1], other_hub).start()
        for c in range(chunks):
            pack(HOME, c, normed)
        matrices(tables.at[NEAR - 1], take_near, give_near, (own,))

        def near_in(c):
            far_copy(NEAR, c, normed, leaf + j).wait_recv()
            far_copy(BEYOND, c, far.at[NEAR - 1], other_hub).start()
            pack(NEAR, c, far.at[NEAR - 1])

        def far_in(r, c):
            far_copy(r, c, normed, other_hub).wait_recv()
            pack(r, c, far.at[r - 1])

        def settle(r):
            for c in range(chunks):
                others(lambda i: go_arrival(r, c, i, own).wait_recv())

        def merge(r, c):
            wait_back(r, c)
            relay_copy(r, c).wait_recv()

            def one(cols):
                far[r - 1, c, :, cols] = dot32(gives[r], backs[r, c, :, cols]).astype(jnp.bfloat16)

            tiles(one)
            slot = 0 if r == ACROSS else 1
            part_copy(slot, c, far.at[r - 1], slot, other_hub).start()

        def pass_on(c):
            wait_back(NEAR, c)
            part_copy(1, c, normed, 1, other_hub).wait_recv()
            far_copy(BEYOND, c, far.at[NEAR - 1], other_hub).wait_send()

            def one(cols):
                total = dot32(give_near[...], backs_near[c, :, cols]) + partial_in[1, c, :, cols].astype(jnp.float32)
                far[NEAR - 1, c, :, cols] = total.astype(jnp.bfloat16)

            tiles(one)
            part_copy(2, c, far.at[NEAR - 1], 1, leaf + j).start()

        near_in(0)
        table_copy(ACROSS, table, other_hub).wait_recv()
        matrices(tables.at[ACROSS - 1], takes.at[ACROSS], gives.at[ACROSS], bases)
        far_in(ACROSS, 0)
        table_copy(BEYOND, table, other_hub).wait_recv()
        matrices(tables.at[BEYOND - 1], takes.at[BEYOND], gives.at[BEYOND], bases)
        near_in(1)
        far_in(BEYOND, 0)
        near_in(2)
        far_in(BEYOND, 1)
        near_in(3)
        for c in range(1, chunks):
            far_copy(ACROSS, c, normed, other_hub).start()
        far_in(BEYOND, 2)
        for load in loads:
            load.wait()
        settle(HOME)
        expert(HOME)
        far_in(BEYOND, 3)
        settle(NEAR)
        expert(NEAR)
        settle(BEYOND)
        expert(BEYOND)
        far_in(ACROSS, 1)
        far_in(ACROSS, 2)
        merge(BEYOND, 0)
        far_in(ACROSS, 3)
        settle(ACROSS)
        expert(ACROSS)
        merge(BEYOND, 1)
        merge(BEYOND, 2)
        pass_on(0)
        merge(BEYOND, 3)
        pass_on(1)
        merge(ACROSS, 0)
        pass_on(2)
        merge(ACROSS, 1)
        merge(ACROSS, 2)
        pass_on(3)
        merge(ACROSS, 3)
        for c in range(chunks):
            wait_back(HOME, c)
            relay_copy(HOME, c).wait_recv()
            part_copy(0, c, normed, 0, other_hub).wait_recv()

            def close(i, carry):
                at = pl.multiple_of(i * TILE, TILE)
                cols = pl.ds(at, TILE)
                total = dot32(gives[HOME], backs[HOME, c, :, cols]) + partial_in[0, c, :, cols].astype(jnp.float32)
                mixed[:, pl.ds(pl.multiple_of(c * step + at, TILE), TILE)] = total.astype(jnp.bfloat16)
                return carry

            lax.fori_loop(0, step // TILE, close, 0)
        table_copy(ACROSS, table, other_hub).wait_send()
        table_copy(BEYOND, table, other_hub).wait_send()
        for c in range(chunks):
            far_copy(ACROSS, c, normed, other_hub).wait_send()
            for k in range(3):
                part_copy(k, c, normed, 0, other_hub).wait_send()
            for r in (HOME, ACROSS, BEYOND):
                everyone(lambda i: go_copy(r, c, 1, i).wait_send())

    def leaf_role():
        table_copy(NEAR, table, hub + j).start()
        for c in range(chunks):
            far_copy(NEAR, c, normed, hub + j).start()
        for load in loads:
            load.start()
        matrices(table, take_near, give_near, (own,))
        for c in range(chunks):
            pack(NEAR, c, normed)
        for load in loads:
            load.wait()
        for c in range(chunks):
            others(lambda i: go_arrival(NEAR, c, i, own).wait_recv())
        expert(NEAR)
        for r in (HOME, BEYOND, ACROSS):
            for c in range(chunks):
                everyone(lambda i: go_arrival(r, c, i, hub).wait_recv())
            expert(r)
            for c in range(chunks):
                wait_back(r, c)
                relay_copy(r, c).start()
        for c in range(chunks):
            wait_back(NEAR, c)
            part_copy(2, c, normed, 1, hub + j).wait_recv()

            def close(i, carry):
                at = pl.multiple_of(i * TILE, TILE)
                cols = pl.ds(at, TILE)
                total = dot32(give_near[...], backs_near[c, :, cols]) + partial_in[1, c, :, cols].astype(jnp.float32)
                mixed[:, pl.ds(pl.multiple_of(c * step + at, TILE), TILE)] = total.astype(jnp.bfloat16)
                return carry

            lax.fori_loop(0, step // TILE, close, 0)
        table_copy(NEAR, table, hub + j).wait_send()
        for c in range(chunks):
            far_copy(NEAR, c, normed, hub + j).wait_send()
            for r in (HOME, ACROSS, BEYOND):
                relay_copy(r, c).wait_send()

    @pl.when(is_hub)
    def _():
        hub_role()

    @pl.when(jnp.logical_not(is_hub))
    def _():
        leaf_role()

    def drain(r):
        for c in range(chunks):
            others(lambda i: back_copy(r, c, i).wait_send())

    for r in range(4):
        drain(r)
    for c in range(chunks):
        others(lambda i: go_copy(NEAR, c, 0, i).wait_send())

    @pl.when(is_hub)
    def _():
        for r in (HOME, ACROSS, BEYOND):
            for c in range(chunks):
                others(lambda i: go_copy(r, c, 0, i).wait_send())


def body(tokens, norm_gain, route_ids, route_gates, w_gate, w_up, w_down):
    rows, width = tokens.shape
    top = route_ids.shape[1]
    devices = lax.axis_size("ep")
    experts = devices
    ff = w_gate.shape[2]
    capacity = 3 * rows * top // (2 * experts)
    m = devices // 4
    unit = m * capacity
    step = width // CHUNKS
    weights = (route_gates / jnp.sum(route_gates, axis=1, keepdims=True)).T
    table = jnp.concatenate([slot_index(route_ids, experts, capacity), weights])
    vmem = pl.BlockSpec(memory_space=pltpu.VMEM)
    hbm = pl.BlockSpec(memory_space=pl.ANY)
    bf16 = jnp.bfloat16
    dma = pltpu.SemaphoreType.DMA
    return pl.pallas_call(
        functools.partial(kernel, devices, capacity, top),
        out_shape=jax.ShapeDtypeStruct((rows, width), bf16),
        in_specs=[hbm, vmem, vmem, hbm, hbm, hbm],
        out_specs=vmem,
        scratch_shapes=[
            pltpu.VMEM((CHUNKS, rows, step), bf16),
            pltpu.VMEM((3, CHUNKS, rows, step), bf16),
            pltpu.VMEM((3, *table.shape), jnp.float32),
            pltpu.VMEM((3, 2 * unit, rows), bf16),
            pltpu.VMEM((3, rows, 2 * unit), bf16),
            pltpu.VMEM((unit, rows), bf16),
            pltpu.VMEM((rows, unit), bf16),
            pltpu.VMEM((3, CHUNKS, 2 * unit, step), bf16),
            pltpu.VMEM((CHUNKS, unit, step), bf16),
            pltpu.VMEM((4, CHUNKS, unit, step), bf16),
            pltpu.VMEM((unit, ff), bf16),
            pltpu.VMEM((width, ff), bf16),
            pltpu.VMEM((width, ff), bf16),
            pltpu.VMEM((ff, width), bf16),
            pltpu.VMEM((3, CHUNKS, 2 * unit, step), bf16),
            pltpu.VMEM((CHUNKS, unit, step), bf16),
            pltpu.VMEM((2, CHUNKS, rows, step), bf16),
            dma((4,)),
            dma((3,)),
            dma((3,)),
            dma((3, CHUNKS)),
            dma((3, CHUNKS)),
            dma((4, CHUNKS, 2 * m)),
            dma((4, CHUNKS, m)),
            dma((4, CHUNKS, m)),
            dma((4, CHUNKS, m)),
            dma((3, CHUNKS)),
            dma((3, CHUNKS)),
            dma((3, CHUNKS)),
            dma((2, CHUNKS)),
        ],
        compiler_params=pltpu.CompilerParams(
            collective_id=0, has_side_effects=True, vmem_limit_bytes=VMEM_BYTES
        ),
    )(tokens, norm_gain[None, :], table, w_gate, w_up, w_down)


def solution(mesh):
    placed = (
        P(("grp", "ep"), None),
        P(),
        P(("grp", "ep"), None),
        P(("grp", "ep"), None),
        P("ep", None, None),
        P("ep", None, None),
        P("ep", None, None),
    )
    return jax.shard_map(
        body, mesh=mesh, in_specs=placed, out_specs=P(("grp", "ep"), None), check_vma=False
    )
```

time: 248 us -> 238 us (0.960)
  Pallas kernels: 239 us -> 231 us
    pallas_call x1, Pallas kernels: 239 us -> 231 us  [body(): pl.pallas_call(functools.partial(kernel, devices, capacity, top), out_sha...]
where the time goes in v1:
time: 238 us; the launch traced here: 237 us
  Pallas kernels  231 us (97%)
  local copies, waits for them, and re-layouts  3.93 us (2%)
    pallas_call x1, Pallas kernels, body(): pl.pallas_call(functools.partial(kernel, devices, capacity, top), out_sha...  231 us

profile of v1, /device:TPU:15, one launch (start us, length us, event | category | flops | bytes accessed | tf_op | source)
XLA Modules:
  0.0 237.2 jit_solution(13683400284887003585)
XLA Ops:
  0.0 0.7 reduce_sum.29
  0.7 0.7 divide_bitcast_fusion
  1.4 0.8 fusion.2
  2.2 0.3 select_reduce_fusion.1
  2.4 0.6 pad_maximum_fusion.table
  3.1 230.9 %shard_map.73 = bf16[512,2048]{1,0:T(8,128)(2,1)} custom-call(bf16[512,2048]{1,0:T(8,128)(2,1)} %tokens_hbm.1, f32[1,2048]{1,0:T(1,128)} %bitcast.7, f32[4,512]{1,0:T(4,128)} %pad_maximum_fusion.table, bf16[1,2048,1024]{2,1,0:T(8,128)(2,1)} %gate_hbm.1, bf16[1,2048,1024]{2,1,0:T(8,128)(2,1)} %up_hbm.1, bf16[1,1024,2048]{2,1,0:T(8,128)(2,1)} %down_hbm.1), custom_call_target="tpu_custom_call" | custom-call | tf_op jit(solution)/shard_map/pallas_call | solution.py:426
  234.0 3.2 %copy.9 = bf16[512,2048]{1,0:T(8,128)(2,1)} copy(bf16[512,2048]{1,0:T(8,128)(2,1)} %shard_map.73) | data formatting | bytes 4194304
  (1 shorter events, 0.0 us)

commit v2 on v1

--- a/solution.py
+++ b/solution.py
@@ -206,7 +206,11 @@
         others(lambda i: go_copy(r, c, 0, i).start())
         arrived[r, c, span(j), :] = target[span(j), :]
 
-    def expert(r):
+    def hand_back(r, c):
+        others(lambda i: back_copy(r, c, i).start())
+        returns(r, c)[span(j), :] = arrived[r, c, span(j), :]
+
+    def expert(r, send):
         def gated(i, carry):
             cols = pl.ds(pl.multiple_of(i * TILE, TILE), TILE)
             gate_pre = dot32(arrived[r, 0], w_gate[0:step, cols])
@@ -227,8 +231,8 @@
                 return carry
 
             lax.fori_loop(0, step // TILE, out, 0)
-            others(lambda i: back_copy(r, c, i).start())
-            returns(r, c)[span(j), :] = arrived[r, c, span(j), :]
+            if send:
+                hand_back(r, c)
 
     def wait_back(r, c):
         others(lambda i: back_arrival(r, c, i).wait_recv())
@@ -285,7 +289,6 @@
         near_in(0)
         table_copy(ACROSS, table, other_hub).wait_recv()
         matrices(tables.at[ACROSS - 1], takes.at[ACROSS], gives.at[ACROSS], bases)
-        far_in(ACROSS, 0)
         table_copy(BEYOND, table, other_hub).wait_recv()
         matrices(tables.at[BEYOND - 1], takes.at[BEYOND], gives.at[BEYOND], bases)
         near_in(1)
@@ -299,23 +302,30 @@
         for load in loads:
             load.wait()
         settle(HOME)
-        expert(HOME)
+        expert(HOME, False)
         far_in(BEYOND, 3)
+        settle(BEYOND)
+        expert(BEYOND, True)
+        far_in(ACROSS, 0)
+        far_in(ACROSS, 1)
         settle(NEAR)
-        expert(NEAR)
-        settle(BEYOND)
-        expert(BEYOND)
-        far_in(ACROSS, 1)
+        expert(NEAR, False)
         far_in(ACROSS, 2)
+        hand_back(NEAR, 0)
+        hand_back(NEAR, 1)
+        far_in(ACROSS, 3)
         merge(BEYOND, 0)
-        far_in(ACROSS, 3)
+        hand_back(NEAR, 2)
+        hand_back(NEAR, 3)
+        merge(BEYOND, 1)
         settle(ACROSS)
-        expert(ACROSS)
-        merge(BEYOND, 1)
+        expert(ACROSS, True)
         merge(BEYOND, 2)
         pass_on(0)
         merge(BEYOND, 3)
         pass_on(1)
+        for c in range(chunks):
+            hand_back(HOME, c)
         merge(ACROSS, 0)
         pass_on(2)
         merge(ACROSS, 1)
@@ -351,20 +361,35 @@
         for load in loads:
             load.start()
         matrices(table, take_near, give_near, (own,))
-        for c in range(chunks):
-            pack(NEAR, c, normed)
         for load in loads:
             load.wait()
-        for c in range(chunks):
-            others(lambda i: go_arrival(NEAR, c, i, own).wait_recv())
-        expert(NEAR)
-        for r in (HOME, BEYOND, ACROSS):
+
+        def settle(r):
             for c in range(chunks):
                 everyone(lambda i: go_arrival(r, c, i, hub).wait_recv())
-            expert(r)
-            for c in range(chunks):
-                wait_back(r, c)
-                relay_copy(r, c).start()
+
+        def send_on(r, c):
+            wait_back(r, c)
+            relay_copy(r, c).start()
+
+        settle(HOME)
+        expert(HOME, True)
+        for c in range(chunks - 1):
+            send_on(HOME, c)
+        settle(BEYOND)
+        expert(BEYOND, True)
+        send_on(HOME, chunks - 1)
+        for c in range(chunks):
+            send_on(BEYOND, c)
+        settle(ACROSS)
+        expert(ACROSS, True)
+        for c in range(chunks):
+            pack(NEAR, c, normed)
+        for c in range(chunks):
+            send_on(ACROSS, c)
+        for c in range(chunks):
+            others(lambda i: go_arrival(NEAR, c, i, own).wait_recv())
+        expert(NEAR, True)
         for c in range(chunks):
             wait_back(NEAR, c)
             part_copy(2, c, normed, 1, hub + j).wait_recv()

time: 238 us -> 210 us (0.88)
  Pallas kernels: 231 us -> 202 us
    pallas_call x1, Pallas kernels: 231 us -> 202 us  [body(): pl.pallas_call(functools.partial(kernel, devices, capacity, top), out_sha...]
where the time goes in v2:
time: 210 us; the launch traced here: 208 us
  Pallas kernels  202 us (96%)
  local copies, waits for them, and re-layouts  3.93 us (2%)
    pallas_call x1, Pallas kernels, body(): pl.pallas_call(functools.partial(kernel, devices, capacity, top), out_sha...  202 us

profile of v2, /device:TPU:15, one launch (start us, length us, event | category | flops | bytes accessed | tf_op | source)
XLA Modules:
  0.0 208.1 jit_solution(9746065610039370157)
XLA Ops:
  0.0 0.7 reduce_sum.29
  0.7 0.7 divide_bitcast_fusion
  1.4 0.8 fusion.2
  2.2 0.3 select_reduce_fusion.1
  2.4 0.6 pad_maximum_fusion.table
  3.1 201.9 %shard_map.73 = bf16[512,2048]{1,0:T(8,128)(2,1)} custom-call(bf16[512,2048]{1,0:T(8,128)(2,1)} %tokens_hbm.1, f32[1,2048]{1,0:T(1,128)} %bitcast.7, f32[4,512]{1,0:T(4,128)} %pad_maximum_fusion.table, bf16[1,2048,1024]{2,1,0:T(8,128)(2,1)} %gate_hbm.1, bf16[1,2048,1024]{2,1,0:T(8,128)(2,1)} %up_hbm.1, bf16[1,1024,2048]{2,1,0:T(8,128)(2,1)} %down_hbm.1), custom_call_target="tpu_custom_call" | custom-call | tf_op jit(solution)/shard_map/pallas_call | solution.py:451
  205.0 3.2 %copy.9 = bf16[512,2048]{1,0:T(8,128)(2,1)} copy(bf16[512,2048]{1,0:T(8,128)(2,1)} %shard_map.73) | data formatting | bytes 4194304
  (1 shorter events, 0.0 us)

commit v3 on v2

v3 whole, which is shorter than its diff:
```python
import functools

import jax
import jax.numpy as jnp
from jax import lax
from jax.experimental import pallas as pl
from jax.experimental.pallas import tpu as pltpu
from jax.sharding import PartitionSpec as P

EPS = 1e-06
CHUNKS = 8
TILE = 256
VMEM_BYTES = 67000000


def dot32(a, b):
    return jnp.dot(a, b, preferred_element_type=jnp.float32)


HOME, ACROSS, BEYOND, NEAR = range(4)


def kernel(
    devices, capacity, top,
    tokens_hbm, gain, route_ids, route_gates, gate_hbm, up_hbm, down_hbm,
    mixed_hbm,
    mixed, table, normed, far, tables, takes, gives, take_near, give_near, packed, packed_near, arrived, hidden,
    w_gate, w_up, w_down, backs, backs_near, partial_in,
    load_sems, table_send, table_recv, far_send, far_recv, go_send, go_recv, back_send, back_recv,
    relay_send, relay_recv, part_send, part_recv, out_sem,
):
    m = devices // 4
    half = 2 * m
    unit = m * capacity
    chunks, rows, step = normed.shape
    ff = w_gate.shape[1]
    me = lax.axis_index("ep")
    side = me // half
    plane = me // m
    j = me % m
    q = me % half
    own = plane * m
    hub = (1 + side) * m
    leaf = 3 * side * m
    other_hub = (2 - side) * m + j
    peer = own + (j + 1) % m
    is_hub = plane * (3 - plane) > 0

    barrier = pltpu.get_barrier_semaphore()

    def greet(i, carry):
        pl.semaphore_signal(barrier, inc=1, device_id={"ep": side * half + (q + 1 + i) % half})
        return carry

    token_load = pltpu.make_async_copy(tokens_hbm, mixed, load_sems.at[3])
    token_load.start()
    lax.fori_loop(0, half - 1, greet, 0)

    @pl.when(is_hub)
    def _():
        pl.semaphore_signal(barrier, inc=1, device_id={"ep": other_hub})

    loads = [
        pltpu.make_async_copy(gate_hbm.at[0], w_gate, load_sems.at[0]),
        pltpu.make_async_copy(up_hbm.at[0], w_up, load_sems.at[1]),
        pltpu.make_async_copy(down_hbm.at[0], w_down, load_sems.at[2]),
    ]
    expert_at = lax.broadcasted_iota(jnp.int32, (devices, rows), 0)
    hits = [route_ids[k : k + 1, :] == expert_at for k in range(top)]
    named = sum(jnp.where(h, 1.0, 0.0) for h in hits)
    earlier = lax.broadcasted_iota(jnp.int32, (rows, rows), 0) < lax.broadcasted_iota(jnp.int32, (rows, rows), 1)
    ranked = dot32(named.astype(jnp.bfloat16), jnp.where(earlier, 1.0, 0.0).astype(jnp.bfloat16))
    base = ranked + (expert_at * capacity).astype(jnp.float32)
    gates = route_gates[...]
    weights = gates / jnp.sum(gates, axis=0, keepdims=True)
    for k in range(top):
        table[k : k + 1, :] = jnp.sum(jnp.where(hits[k], base, 0.0), axis=0, keepdims=True)
        table[top + k : top + k + 1, :] = weights[k : k + 1, :]
    token_load.wait()

    def norm(i, carry):
        at = pl.ds(pl.multiple_of(i * 64, 64), 64)
        floats = mixed[at, :].astype(jnp.float32)
        scale = lax.rsqrt(jnp.mean(floats * floats, axis=-1, keepdims=True) + EPS)
        value = (floats * scale * gain[...]).astype(jnp.bfloat16)
        for c in range(chunks):
            normed[c, at, :] = value[:, c * step : (c + 1) * step]
        return carry

    lax.fori_loop(0, rows // 64, norm, 0)

    @pl.when(is_hub)
    def _():
        pl.semaphore_wait(barrier, half)

    @pl.when(jnp.logical_not(is_hub))
    def _():
        pl.semaphore_wait(barrier, half - 1)

    def remote(src, dst, send, recv, device):
        return pltpu.make_async_remote_copy(
            src_ref=src, dst_ref=dst, send_sem=send, recv_sem=recv, device_id={"ep": device}
        )

    def table_copy(r, src, device):
        return remote(src, tables.at[r - 1], table_send.at[r - 1], table_recv.at[r - 1], device)

    def far_copy(r, c, src, device):
        return remote(src.at[c], far.at[r - 1, c], far_send.at[r - 1], far_recv.at[r - 1, c], device)

    def part_copy(k, c, src, slot, device):
        return remote(src.at[c], partial_in.at[slot, c], part_send.at[k], part_recv.at[slot, c], device)

    def span(i, part=0):
        return pl.ds(pl.multiple_of(part * unit + i * capacity, 16), capacity)

    def packs(r, c):
        return packed_near.at[c] if r == NEAR else packed.at[r, c]

    def returns(r, c):
        return backs_near.at[c] if r == NEAR else backs.at[r, c]

    def go_copy(r, c, part, i):
        target = (leaf if part else own) + i
        return remote(
            packs(r, c).at[span(i, part)], arrived.at[r, c, span(j)],
            go_send.at[r], go_recv.at[r], target,
        )

    def settle(r, every):
        count = unit if every else unit - capacity
        got = arrived.at[r, :, pl.ds(0, count)]
        remote(got, got, go_send.at[r], go_recv.at[r], peer).wait_recv()

    def go_sent(r):
        sent = packed_near.at[:, pl.ds(0, unit - capacity)] if r == NEAR else packed.at[r, :, pl.ds(0, 2 * unit - capacity)]
        remote(sent, sent, go_send.at[r], go_recv.at[r], peer).wait_send()

    def back_copy(r, c, i):
        return remote(
            arrived.at[r, c, span(i)], returns(r, c).at[span(j)],
            back_send.at[r], back_recv.at[r, c], own + i,
        )

    def back_sent(r):
        sent = arrived.at[r, :, pl.ds(0, unit - capacity)]
        remote(sent, sent, back_send.at[r], go_recv.at[r], peer).wait_send()

    def relay_copy(r, c):
        return remote(
            backs.at[r, c, pl.ds(0, unit)], backs.at[r, c, pl.ds(unit, unit)],
            relay_send.at[r], relay_recv.at[r, c], hub + j,
        )

    def others(act):
        def one(i, carry):
            act((j + 1 + i) % m)
            return carry

        lax.fori_loop(0, m - 1, one, 0)

    def everyone(act):
        def one(i, carry):
            act((j + i) % m)
            return carry

        lax.fori_loop(0, m, one, 0)

    def matrices(source, take, give, bases):
        width = 128

        def block(part, first):
            def one(i, carry):
                at = pl.multiple_of(part * unit + i * width, width)
                start = first * capacity + i * width
                slots = (start + lax.broadcasted_iota(jnp.int32, (width, rows), 0)).astype(jnp.float32)
                taken = jnp.zeros((width, rows), jnp.float32)
                total = jnp.zeros((width, rows), jnp.float32)
                for k in range(top):
                    hit = source[k : k + 1, :] == slots
                    taken = taken + jnp.where(hit, 1.0, 0.0)
                    total = total + jnp.where(hit, source[top + k : top + k + 1, :], 0.0)
                take[pl.ds(at, width), :] = taken.astype(jnp.bfloat16)
                give[:, pl.ds(at, width)] = total.T.astype(jnp.bfloat16)
                return carry

            lax.fori_loop(0, unit // width, one, 0)

        for part, first in enumerate(bases):
            block(part, first)

    def each(low, high, act):
        def one(c, carry):
            act(c)
            return carry

        lax.fori_loop(low, high, one, 0)

    def pack(r, c, source):
        take = take_near if r == NEAR else takes.at[r]
        target = packs(r, c)

        target[...] = dot32(take[...], source[c]).astype(jnp.bfloat16)
        if r != NEAR:
            everyone(lambda i: go_copy(r, c, 1, i).start())
        others(lambda i: go_copy(r, c, 0, i).start())
        arrived[r, c, span(j), :] = target[span(j), :]

    def hand_back(r, c):
        others(lambda i: back_copy(r, c, i).start())
        returns(r, c)[span(j), :] = arrived[r, c, span(j), :]

    def expert(r, send):
        def gated(i, carry):
            cols = pl.ds(pl.multiple_of(i * TILE, TILE), TILE)
            gate_pre = dot32(arrived[r, 0], w_gate[0:step, cols])
            up_pre = dot32(arrived[r, 0], w_up[0:step, cols])
            for c in range(1, chunks):
                gate_pre += dot32(arrived[r, c], w_gate[c * step : (c + 1) * step, cols])
                up_pre += dot32(arrived[r, c], w_up[c * step : (c + 1) * step, cols])
            hidden[:, cols] = (gate_pre / (1.0 + jnp.exp(-gate_pre)) * up_pre).astype(jnp.bfloat16)
            return carry

        lax.fori_loop(0, ff // TILE, gated, 0)

        def out(c):
            cols = pl.ds(pl.multiple_of(c * step, step), step)
            arrived[r, c] = dot32(hidden[...], w_down[:, cols]).astype(jnp.bfloat16)
            if send:
                hand_back(r, c)

        each(0, chunks, out)

    def out_copy(c):
        cols = pl.ds(pl.multiple_of(c * step, step), step)
        return pltpu.make_async_copy(mixed.at[:, cols], mixed_hbm.at[:, cols], out_sem)

    def finish(c, total):
        mixed[:, pl.ds(pl.multiple_of(c * step, step), step)] = total.astype(jnp.bfloat16)
        out_copy(c).start()

    def wait_back(r, c):
        got = returns(r, c).at[pl.ds(0, unit - capacity)]
        remote(got, got, back_send.at[r], back_recv.at[r, c], peer).wait_recv()

    def all_sent(sem, ref):
        remote(ref, ref, sem, go_recv.at[0], peer).wait_send()

    def hub_role():
        bases = (hub, leaf)
        lead = 2
        mid = chunks // 2

        def across_out(c):
            far_copy(ACROSS, c, normed, other_hub).start()

        each(0, lead, across_out)
        table_copy(ACROSS, table, other_hub).start()
        for load in loads:
            load.start()
        matrices(table, takes.at[HOME], gives.at[HOME], bases)
        table_copy(NEAR, table, leaf + j).wait_recv()
        table_copy(BEYOND, tables.at[NEAR - 1], other_hub).start()
        each(0, chunks, lambda c: pack(HOME, c, normed))
        matrices(tables.at[NEAR - 1], take_near, give_near, (own,))

        def near_in(c):
            far_copy(NEAR, c, normed, leaf + j).wait_recv()
            far_copy(BEYOND, c, far.at[NEAR - 1], other_hub).start()
            pack(NEAR, c, far.at[NEAR - 1])

        def far_in(r, c):
            far_copy(r, c, normed, other_hub).wait_recv()
            pack(r, c, far.at[r - 1])

        def merge(r, c):
            wait_back(r, c)
            relay_copy(r, c).wait_recv()
            far[r - 1, c] = dot32(gives[r], backs[r, c]).astype(jnp.bfloat16)
            slot = 0 if r == ACROSS else 1
            part_copy(slot, c, far.at[r - 1], slot, other_hub).start()

        def pass_on(c):
            wait_back(NEAR, c)
            part_copy(1, c, normed, 1, other_hub).wait_recv()
            total = dot32(give_near[...], backs_near[c]) + partial_in[1, c].astype(jnp.float32)
            far[NEAR - 1, c] = total.astype(jnp.bfloat16)
            part_copy(2, c, far.at[NEAR - 1], 1, leaf + j).start()

        def beyond_in(c):
            far_in(BEYOND, c)

        def across_in(c):
            far_in(ACROSS, c)

        each(0, lead, near_in)
        table_copy(ACROSS, table, other_hub).wait_recv()
        matrices(tables.at[ACROSS - 1], takes.at[ACROSS], gives.at[ACROSS], bases)
        table_copy(BEYOND, table, other_hub).wait_recv()
        matrices(tables.at[BEYOND - 1], takes.at[BEYOND], gives.at[BEYOND], bases)

        def early(c):
            beyond_in(c)
            near_in(c + lead)

        each(0, chunks - lead, early)
        each(lead, chunks, across_out)
        for load in loads:
            load.wait()
        settle(HOME, False)
        expert(HOME, False)
        each(chunks - lead, chunks, beyond_in)
        each(0, lead, across_in)
        settle(NEAR, False)
        expert(NEAR, False)
        settle(BEYOND, False)
        expert(BEYOND, True)
        each(lead, mid + 1, across_in)
        each(mid + 1, chunks - 1, across_in)
        merge(BEYOND, 0)
        across_in(chunks - 1)
        each(0, chunks, lambda c: hand_back(NEAR, c))
        each(1, mid, lambda c: merge(BEYOND, c))
        all_sent(far_send.at[BEYOND - 1], far.at[NEAR - 1])
        settle(ACROSS, False)
        expert(ACROSS, True)
        each(mid, chunks, lambda c: merge(BEYOND, c))
        each(0, chunks, lambda c: hand_back(HOME, c))
        each(0, mid, pass_on)

        def late(c):
            pass_on(c)
            merge(ACROSS, c - mid)

        each(mid, chunks, late)
        each(mid, chunks, lambda c: merge(ACROSS, c))
        all_sent(table_send.at[ACROSS - 1], table)
        all_sent(table_send.at[BEYOND - 1], table)
        all_sent(far_send.at[ACROSS - 1], normed)
        for r in range(4):
            go_sent(r)
            back_sent(r)

        def close(c):
            wait_back(HOME, c)
            relay_copy(HOME, c).wait_recv()
            part_copy(0, c, normed, 0, other_hub).wait_recv()
            finish(c, dot32(gives[HOME], backs[HOME, c]) + partial_in[0, c].astype(jnp.float32))

        each(0, chunks, close)
        for k in range(3):
            all_sent(part_send.at[k], normed)

    def leaf_role():
        lag = 2
        table_copy(NEAR, table, hub + j).start()
        each(0, chunks, lambda c: far_copy(NEAR, c, normed, hub + j).start())
        for load in loads:
            load.start()
        matrices(table, take_near, give_near, (own,))
        for load in loads:
            load.wait()

        def send_on(r, c):
            wait_back(r, c)
            relay_copy(r, c).start()

        settle(HOME, True)
        expert(HOME, True)
        each(0, chunks - lag, lambda c: send_on(HOME, c))
        settle(BEYOND, True)
        expert(BEYOND, True)
        each(0, chunks, lambda c: send_on(BEYOND, c))
        each(chunks - lag, chunks, lambda c: send_on(HOME, c))
        settle(ACROSS, True)
        expert(ACROSS, True)
        each(0, chunks, lambda c: pack(NEAR, c, normed))
        each(0, chunks, lambda c: send_on(ACROSS, c))
        settle(NEAR, False)
        expert(NEAR, True)
        all_sent(table_send.at[NEAR - 1], table)
        all_sent(far_send.at[NEAR - 1], normed)

        def close(c):
            wait_back(NEAR, c)
            part_copy(2, c, normed, 1, hub + j).wait_recv()
            finish(c, dot32(give_near[...], backs_near[c]) + partial_in[1, c].astype(jnp.float32))

        each(0, chunks, close)
        go_sent(NEAR)
        for r in range(4):
            back_sent(r)
        for r in (HOME, ACROSS, BEYOND):
            all_sent(relay_send.at[r], backs.at[r, :, pl.ds(0, unit)])

    @pl.when(is_hub)
    def _():
        hub_role()

    @pl.when(jnp.logical_not(is_hub))
    def _():
        leaf_role()

    pltpu.make_async_copy(mixed, mixed_hbm, out_sem).wait()


def body(tokens, norm_gain, route_ids, route_gates, w_gate, w_up, w_down):
    rows, width = tokens.shape
    top = route_ids.shape[1]
    devices = lax.axis_size("ep")
    experts = devices
    ff = w_gate.shape[2]
    capacity = 3 * rows * top // (2 * experts)
    m = devices // 4
    unit = m * capacity
    step = width // CHUNKS
    vmem = pl.BlockSpec(memory_space=pltpu.VMEM)
    hbm = pl.BlockSpec(memory_space=pl.ANY)
    bf16 = jnp.bfloat16
    dma = pltpu.SemaphoreType.DMA
    return pl.pallas_call(
        functools.partial(kernel, devices, capacity, top),
        out_shape=jax.ShapeDtypeStruct((rows, width), bf16),
        in_specs=[hbm, vmem, vmem, vmem, hbm, hbm, hbm],
        out_specs=hbm,
        scratch_shapes=[
            pltpu.VMEM((rows, width), bf16),
            pltpu.VMEM((2 * top, rows), jnp.float32),
            pltpu.VMEM((CHUNKS, rows, step), bf16),
            pltpu.VMEM((3, CHUNKS, rows, step), bf16),
            pltpu.VMEM((3, 2 * top, rows), jnp.float32),
            pltpu.VMEM((3, 2 * unit, rows), bf16),
            pltpu.VMEM((3, rows, 2 * unit), bf16),
            pltpu.VMEM((unit, rows), bf16),
            pltpu.VMEM((rows, unit), bf16),
            pltpu.VMEM((3, CHUNKS, 2 * unit, step), bf16),
            pltpu.VMEM((CHUNKS, unit, step), bf16),
            pltpu.VMEM((4, CHUNKS, unit, step), bf16),
            pltpu.VMEM((unit, ff), bf16),
            pltpu.VMEM((width, ff), bf16),
            pltpu.VMEM((width, ff), bf16),
            pltpu.VMEM((ff, width), bf16),
            pltpu.VMEM((3, CHUNKS, 2 * unit, step), bf16),
            pltpu.VMEM((CHUNKS, unit, step), bf16),
            pltpu.VMEM((2, CHUNKS, rows, step), bf16),
            dma((4,)),
            dma((3,)),
            dma((3,)),
            dma((3,)),
            dma((3, CHUNKS)),
            dma((4,)),
            dma((4,)),
            dma((4,)),
            dma((4, CHUNKS)),
            dma((3,)),
            dma((3, CHUNKS)),
            dma((3,)),
            dma((2, CHUNKS)),
            dma,
        ],
        compiler_params=pltpu.CompilerParams(
            collective_id=0, has_side_effects=True, vmem_limit_bytes=VMEM_BYTES
        ),
    )(tokens, norm_gain[None, :], route_ids.T, route_gates.T, w_gate, w_up, w_down)


def solution(mesh):
    placed = (
        P(("grp", "ep"), None),
        P(),
        P(("grp", "ep"), None),
        P(("grp", "ep"), None),
        P("ep", None, None),
        P("ep", None, None),
        P("ep", None, None),
    )
    return jax.shard_map(
        body, mesh=mesh, in_specs=placed, out_specs=P(("grp", "ep"), None), check_vma=False
    )
```

time: 210 us -> 193 us (0.919)
  Pallas kernels: 202 us -> 190 us
    pallas_call x1, Pallas kernels: 202 us -> 190 us  [body(): pl.pallas_call(functools.partial(kernel, devices, capacity, top), out_sha...]
where the time goes in v3:
time: 193 us
  Pallas kernels  190 us (98%)
  local copies, waits for them, and re-layouts  3.16 us (2%)
    pallas_call x1, Pallas kernels, body(): pl.pallas_call(functools.partial(kernel, devices, capacity, top), out_sha...  190 us

profile of v3, /device:TPU:15, one launch (start us, length us, event | category | flops | bytes accessed | tf_op | source)
XLA Modules:
  0.0 192.7 jit_solution(4798399238541864147)
XLA Ops:
  0.0 189.5 %shard_map.73 = bf16[512,2048]{1,0:T(8,128)(2,1)} custom-call(bf16[512,2048]{1,0:T(8,128)(2,1)} %tokens_hbm.1, f32[1,2048]{1,0:T(1,128)} %bitcast.3, s32[2,512]{1,0:T(2,128)} %bitcast.4, f32[2,512]{1,0:T(2,128)} %bitcast.5, bf16[1,2048,1024]{2,1,0:T(8,128)(2,1)} %gate_hbm.1, bf16[1,2048,1024]{2,1,0:T(8,128)(2,1)} %up_hbm.1, bf16[1,1024,2048]{2,1,0:T(8,128)(2,1)} %down_hbm.1), custom_call_target="tpu_custom_call" | custom-call | tf_op jit(solution)/shard_map/pallas_call | solution.py:421
  189.5 3.2 %copy.9 = bf16[512,2048]{1,0:T(8,128)(2,1)} copy(bf16[512,2048]{1,0:T(8,128)(2,1)} %shard_map.73) | data formatting | bytes 4194304

commit v4 on v3

--- a/solution.py
+++ b/solution.py
@@ -10,7 +10,7 @@
 EPS = 1e-06
 CHUNKS = 8
 TILE = 256
-VMEM_BYTES = 67000000
+VMEM_BYTES = 62000000
 
 
 def dot32(a, b):
@@ -22,17 +22,17 @@
 
 def kernel(
     devices, capacity, top,
-    tokens_hbm, gain, route_ids, route_gates, gate_hbm, up_hbm, down_hbm,
-    mixed_hbm,
-    mixed, table, normed, far, tables, takes, gives, take_near, give_near, packed, packed_near, arrived, hidden,
+    tokens_hbm, gain_hbm, ids_hbm, gates_hbm, gate_hbm, up_hbm, down_hbm,
+    mixed,
+    gain, route_ids, route_gates, table, far, tables, takes, gives, take_near, give_near, packed, packed_near, arrived, hidden,
     w_gate, w_up, w_down, backs, backs_near, partial_in,
     load_sems, table_send, table_recv, far_send, far_recv, go_send, go_recv, back_send, back_recv,
-    relay_send, relay_recv, part_send, part_recv, out_sem,
+    relay_send, relay_recv, part_send, part_recv,
 ):
     m = devices // 4
     half = 2 * m
     unit = m * capacity
-    chunks, rows, step = normed.shape
+    _, chunks, rows, step = far.shape
     ff = w_gate.shape[1]
     me = lax.axis_index("ep")
     side = me // half
@@ -53,7 +53,14 @@
         return carry
 
     token_load = pltpu.make_async_copy(tokens_hbm, mixed, load_sems.at[3])
+    small_loads = [
+        pltpu.make_async_copy(ids_hbm, route_ids, load_sems.at[4]),
+        pltpu.make_async_copy(gates_hbm, route_gates, load_sems.at[5]),
+        pltpu.make_async_copy(gain_hbm, gain, load_sems.at[6]),
+    ]
     token_load.start()
+    for load in small_loads:
+        load.start()
     lax.fori_loop(0, half - 1, greet, 0)
 
     @pl.when(is_hub)
@@ -65,29 +72,7 @@
         pltpu.make_async_copy(up_hbm.at[0], w_up, load_sems.at[1]),
         pltpu.make_async_copy(down_hbm.at[0], w_down, load_sems.at[2]),
     ]
-    expert_at = lax.broadcasted_iota(jnp.int32, (devices, rows), 0)
-    hits = [route_ids[k : k + 1, :] == expert_at for k in range(top)]
-    named = sum(jnp.where(h, 1.0, 0.0) for h in hits)
-    earlier = lax.broadcasted_iota(jnp.int32, (rows, rows), 0) < lax.broadcasted_iota(jnp.int32, (rows, rows), 1)
-    ranked = dot32(named.astype(jnp.bfloat16), jnp.where(earlier, 1.0, 0.0).astype(jnp.bfloat16))
-    base = ranked + (expert_at * capacity).astype(jnp.float32)
-    gates = route_gates[...]
-    weights = gates / jnp.sum(gates, axis=0, keepdims=True)
-    for k in range(top):
-        table[k : k + 1, :] = jnp.sum(jnp.where(hits[k], base, 0.0), axis=0, keepdims=True)
-        table[top + k : top + k + 1, :] = weights[k : k + 1, :]
     token_load.wait()
-
-    def norm(i, carry):
-        at = pl.ds(pl.multiple_of(i * 64, 64), 64)
-        floats = mixed[at, :].astype(jnp.float32)
-        scale = lax.rsqrt(jnp.mean(floats * floats, axis=-1, keepdims=True) + EPS)
-        value = (floats * scale * gain[...]).astype(jnp.bfloat16)
-        for c in range(chunks):
-            normed[c, at, :] = value[:, c * step : (c + 1) * step]
-        return carry
-
-    lax.fori_loop(0, rows // 64, norm, 0)
 
     @pl.when(is_hub)
     def _():
@@ -102,11 +87,14 @@
             src_ref=src, dst_ref=dst, send_sem=send, recv_sem=recv, device_id={"ep": device}
         )
 
+    def raw(c):
+        return mixed.at[:, pl.ds(pl.multiple_of(c * step, step), step)]
+
     def table_copy(r, src, device):
         return remote(src, tables.at[r - 1], table_send.at[r - 1], table_recv.at[r - 1], device)
 
     def far_copy(r, c, src, device):
-        return remote(src.at[c], far.at[r - 1, c], far_send.at[r - 1], far_recv.at[r - 1, c], device)
+        return remote(src, far.at[r - 1, c], far_send.at[r - 1], far_recv.at[r - 1, c], device)
 
     def part_copy(k, c, src, slot, device):
         return remote(src.at[c], partial_in.at[slot, c], part_send.at[k], part_recv.at[slot, c], device)
@@ -189,6 +177,21 @@
         for part, first in enumerate(bases):
             block(part, first)
 
+    def build_table():
+        for load in small_loads:
+            load.wait()
+        expert_at = lax.broadcasted_iota(jnp.int32, (devices, rows), 0)
+        hits = [route_ids[k : k + 1, :] == expert_at for k in range(top)]
+        named = sum(jnp.where(h, 1.0, 0.0) for h in hits)
+        earlier = lax.broadcasted_iota(jnp.int32, (rows, rows), 0) < lax.broadcasted_iota(jnp.int32, (rows, rows), 1)
+        ranked = dot32(named.astype(jnp.bfloat16), jnp.where(earlier, 1.0, 0.0).astype(jnp.bfloat16))
+        base = ranked + (expert_at * capacity).astype(jnp.float32)
+        gates = route_gates[...]
+        weights = gates / jnp.sum(gates, axis=0, keepdims=True)
+        for k in range(top):
+            table[k : k + 1, :] = jnp.sum(jnp.where(hits[k], base, 0.0), axis=0, keepdims=True)
+            table[top + k : top + k + 1, :] = weights[k : k + 1, :]
+
     def each(low, high, act):
         def one(c, carry):
             act(c)
@@ -200,7 +203,7 @@
         take = take_near if r == NEAR else takes.at[r]
         target = packs(r, c)
 
-        target[...] = dot32(take[...], source[c]).astype(jnp.bfloat16)
+        target[...] = dot32(take[...], source[...]).astype(jnp.bfloat16)
         if r != NEAR:
             everyone(lambda i: go_copy(r, c, 1, i).start())
         others(lambda i: go_copy(r, c, 0, i).start())
@@ -210,7 +213,27 @@
         others(lambda i: back_copy(r, c, i).start())
         returns(r, c)[span(j), :] = arrived[r, c, span(j), :]
 
+    def norm(r):
+        block = 64
+
+        def some(i, carry):
+            at = pl.ds(pl.multiple_of(i * block, block), block)
+            total = jnp.zeros((block, 1), jnp.float32)
+            for c in range(chunks):
+                floats = arrived[r, c, at, :].astype(jnp.float32)
+                total += jnp.sum(floats * floats, axis=-1, keepdims=True)
+            scale = lax.rsqrt(total / (chunks * step) + EPS)
+            for c in range(chunks):
+                floats = arrived[r, c, at, :].astype(jnp.float32)
+                value = floats * scale * gain[:, c * step : (c + 1) * step]
+                arrived[r, c, at, :] = value.astype(jnp.bfloat16)
+            return carry
+
+        lax.fori_loop(0, unit // block, some, 0)
+
     def expert(r, send):
+        norm(r)
+
         def gated(i, carry):
             cols = pl.ds(pl.multiple_of(i * TILE, TILE), TILE)
             gate_pre = dot32(arrived[r, 0], w_gate[0:step, cols])
@@ -231,13 +254,8 @@
 
         each(0, chunks, out)
 
-    def out_copy(c):
-        cols = pl.ds(pl.multiple_of(c * step, step), step)
-        return pltpu.make_async_copy(mixed.at[:, cols], mixed_hbm.at[:, cols], out_sem)
-
     def finish(c, total):
         mixed[:, pl.ds(pl.multiple_of(c * step, step), step)] = total.astype(jnp.bfloat16)
-        out_copy(c).start()
 
     def wait_back(r, c):
         got = returns(r, c).at[pl.ds(0, unit - capacity)]
@@ -252,26 +270,28 @@
         mid = chunks // 2
 
         def across_out(c):
-            far_copy(ACROSS, c, normed, other_hub).start()
-
-        each(0, lead, across_out)
+            far_copy(ACROSS, c, raw(c), other_hub).start()
+
+        across_out(0)
+        build_table()
         table_copy(ACROSS, table, other_hub).start()
+        each(1, lead, across_out)
         for load in loads:
             load.start()
         matrices(table, takes.at[HOME], gives.at[HOME], bases)
+        each(0, chunks, lambda c: pack(HOME, c, raw(c)))
         table_copy(NEAR, table, leaf + j).wait_recv()
         table_copy(BEYOND, tables.at[NEAR - 1], other_hub).start()
-        each(0, chunks, lambda c: pack(HOME, c, normed))
         matrices(tables.at[NEAR - 1], take_near, give_near, (own,))
 
         def near_in(c):
-            far_copy(NEAR, c, normed, leaf + j).wait_recv()
-            far_copy(BEYOND, c, far.at[NEAR - 1], other_hub).start()
-            pack(NEAR, c, far.at[NEAR - 1])
+            far_copy(NEAR, c, raw(c), leaf + j).wait_recv()
+            far_copy(BEYOND, c, far.at[NEAR - 1, c], other_hub).start()
+            pack(NEAR, c, far.at[NEAR - 1, c])
 
         def far_in(r, c):
-            far_copy(r, c, normed, other_hub).wait_recv()
-            pack(r, c, far.at[r - 1])
+            far_copy(r, c, raw(c), other_hub).wait_recv()
+            pack(r, c, far.at[r - 1, c])
 
         def merge(r, c):
             wait_back(r, c)
@@ -282,7 +302,7 @@
 
         def pass_on(c):
             wait_back(NEAR, c)
-            part_copy(1, c, normed, 1, other_hub).wait_recv()
+            part_copy(1, c, far.at[0], 1, other_hub).wait_recv()
             total = dot32(give_near[...], backs_near[c]) + partial_in[1, c].astype(jnp.float32)
             far[NEAR - 1, c] = total.astype(jnp.bfloat16)
             part_copy(2, c, far.at[NEAR - 1], 1, leaf + j).start()
@@ -320,11 +340,11 @@
         merge(BEYOND, 0)
         across_in(chunks - 1)
         each(0, chunks, lambda c: hand_back(NEAR, c))
-        each(1, mid, lambda c: merge(BEYOND, c))
+        each(1, mid + lead, lambda c: merge(BEYOND, c))
         all_sent(far_send.at[BEYOND - 1], far.at[NEAR - 1])
         settle(ACROSS, False)
         expert(ACROSS, True)
-        each(mid, chunks, lambda c: merge(BEYOND, c))
+        each(mid + lead, chunks, lambda c: merge(BEYOND, c))
         each(0, chunks, lambda c: hand_back(HOME, c))
         each(0, mid, pass_on)
 
@@ -336,7 +356,7 @@
         each(mid, chunks, lambda c: merge(ACROSS, c))
         all_sent(table_send.at[ACROSS - 1], table)
         all_sent(table_send.at[BEYOND - 1], table)
-        all_sent(far_send.at[ACROSS - 1], normed)
+        all_sent(far_send.at[ACROSS - 1], mixed)
         for r in range(4):
             go_sent(r)
             back_sent(r)
@@ -344,17 +364,19 @@
         def close(c):
             wait_back(HOME, c)
             relay_copy(HOME, c).wait_recv()
-            part_copy(0, c, normed, 0, other_hub).wait_recv()
+            part_copy(0, c, far.at[0], 0, other_hub).wait_recv()
             finish(c, dot32(gives[HOME], backs[HOME, c]) + partial_in[0, c].astype(jnp.float32))
 
         each(0, chunks, close)
         for k in range(3):
-            all_sent(part_send.at[k], normed)
+            all_sent(part_send.at[k], far.at[0])
 
     def leaf_role():
         lag = 2
+        far_copy(NEAR, 0, raw(0), hub + j).start()
+        build_table()
         table_copy(NEAR, table, hub + j).start()
-        each(0, chunks, lambda c: far_copy(NEAR, c, normed, hub + j).start())
+        each(1, chunks, lambda c: far_copy(NEAR, c, raw(c), hub + j).start())
         for load in loads:
             load.start()
         matrices(table, take_near, give_near, (own,))
@@ -374,16 +396,16 @@
         each(chunks - lag, chunks, lambda c: send_on(HOME, c))
         settle(ACROSS, True)
         expert(ACROSS, True)
-        each(0, chunks, lambda c: pack(NEAR, c, normed))
+        each(0, chunks, lambda c: pack(NEAR, c, raw(c)))
         each(0, chunks, lambda c: send_on(ACROSS, c))
         settle(NEAR, False)
         expert(NEAR, True)
         all_sent(table_send.at[NEAR - 1], table)
-        all_sent(far_send.at[NEAR - 1], normed)
+        all_sent(far_send.at[NEAR - 1], mixed)
 
         def close(c):
             wait_back(NEAR, c)
-            part_copy(2, c, normed, 1, hub + j).wait_recv()
+            part_copy(2, c, far.at[0], 1, hub + j).wait_recv()
             finish(c, dot32(give_near[...], backs_near[c]) + partial_in[1, c].astype(jnp.float32))
 
         each(0, chunks, close)
@@ -400,8 +422,6 @@
     @pl.when(jnp.logical_not(is_hub))
     def _():
         leaf_role()
-
-    pltpu.make_async_copy(mixed, mixed_hbm, out_sem).wait()
 
 
 def body(tokens, norm_gain, route_ids, route_gates, w_gate, w_up, w_down):
@@ -414,19 +434,19 @@
     m = devices // 4
     unit = m * capacity
     step = width // CHUNKS
-    vmem = pl.BlockSpec(memory_space=pltpu.VMEM)
     hbm = pl.BlockSpec(memory_space=pl.ANY)
     bf16 = jnp.bfloat16
     dma = pltpu.SemaphoreType.DMA
     return pl.pallas_call(
         functools.partial(kernel, devices, capacity, top),
-        out_shape=jax.ShapeDtypeStruct((rows, width), bf16),
-        in_specs=[hbm, vmem, vmem, vmem, hbm, hbm, hbm],
-        out_specs=hbm,
+        out_shape=pltpu.VMEM((rows, width), bf16),
+        in_specs=[hbm] * 7,
+        out_specs=pl.BlockSpec(memory_space=pltpu.VMEM),
         scratch_shapes=[
-            pltpu.VMEM((rows, width), bf16),
+            pltpu.VMEM((1, width), jnp.float32),
+            pltpu.VMEM((top, rows), jnp.int32),
+            pltpu.VMEM((top, rows), jnp.float32),
             pltpu.VMEM((2 * top, rows), jnp.float32),
-            pltpu.VMEM((CHUNKS, rows, step), bf16),
             pltpu.VMEM((3, CHUNKS, rows, step), bf16),
             pltpu.VMEM((3, 2 * top, rows), jnp.float32),
             pltpu.VMEM((3, 2 * unit, rows), bf16),
@@ -443,7 +463,7 @@
             pltpu.VMEM((3, CHUNKS, 2 * unit, step), bf16),
             pltpu.VMEM((CHUNKS, unit, step), bf16),
             pltpu.VMEM((2, CHUNKS, rows, step), bf16),
-            dma((4,)),
+            dma((7,)),
             dma((3,)),
             dma((3,)),
             dma((3,)),
@@ -456,7 +476,6 @@
             dma((3, CHUNKS)),
             dma((3,)),
             dma((2, CHUNKS)),
-            dma,
         ],
         compiler_params=pltpu.CompilerParams(
             collective_id=0, has_side_effects=True, vmem_limit_bytes=VMEM_BYTES

time: 193 us -> 188 us (0.974)
  Pallas kernels: 190 us -> 186 us
    pallas_call x1, Pallas kernels: 190 us -> 186 us  [body(): pl.pallas_call(functools.partial(kernel, devices, capacity, top), out_sha...]
where the time goes in v4:
time: 188 us; the launch traced here: 187 us
  Pallas kernels  186 us (99%)
    pallas_call x1, Pallas kernels, body(): pl.pallas_call(functools.partial(kernel, devices, capacity, top), out_sha...  186 us

profile of v4, /device:TPU:15, one launch (start us, length us, event | category | flops | bytes accessed | tf_op | source)
XLA Modules:
  0.0 187.0 jit_solution(1256100597254729544)
XLA Ops:
  0.0 185.6 %shard_map.73 = bf16[512,2048]{1,0:T(8,128)(2,1)S(1)} custom-call(bf16[512,2048]{1,0:T(8,128)(2,1)} %tokens_hbm.1, f32[1,2048]{1,0:T(1,128)} %bitcast.3, s32[2,512]{1,0:T(2,128)} %bitcast.4, f32[2,512]{1,0:T(2,128)} %bitcast.5, bf16[1,2048,1024]{2,1,0:T(8,128)(2,1)} %gate_hbm.1, bf16[1,2048,1024]{2,1,0:T(8,128)(2,1)} %up_hbm.1, bf16[1,1024,2048]{2,1,0:T(8,128)(2,1)} %down_hbm.1), custom_call_target="tpu_custom_call" | custom-call | tf_op jit(solution)/shard_map/pallas_call | solution.py:440
  185.7 1.3 copy.9

commit v5 on v4

--- a/solution.py
+++ b/solution.py
@@ -25,9 +25,9 @@
     tokens_hbm, gain_hbm, ids_hbm, gates_hbm, gate_hbm, up_hbm, down_hbm,
     mixed,
     gain, route_ids, route_gates, table, far, tables, takes, gives, take_near, give_near, packed, packed_near, arrived, hidden,
-    w_gate, w_up, w_down, backs, backs_near, partial_in,
+    w_gate, w_up, w_down, backs, backs_near, partial_in, local,
     load_sems, table_send, table_recv, far_send, far_recv, go_send, go_recv, back_send, back_recv,
-    relay_send, relay_recv, part_send, part_recv,
+    relay_send, relay_recv, part_send, part_recv, ready,
 ):
     m = devices // 4
     half = 2 * m
@@ -48,35 +48,45 @@
 
     barrier = pltpu.get_barrier_semaphore()
 
+    @pl.when(is_hub)
+    def _():
+        pl.semaphore_signal(barrier, inc=1, device_id={"ep": other_hub})
+
     def greet(i, carry):
-        pl.semaphore_signal(barrier, inc=1, device_id={"ep": side * half + (q + 1 + i) % half})
+        pl.semaphore_signal(barrier, inc=1, device_id={"ep": leaf + (j + 1 + i) % m})
         return carry
 
-    token_load = pltpu.make_async_copy(tokens_hbm, mixed, load_sems.at[3])
+    first_load = pltpu.make_async_copy(tokens_hbm.at[:, pl.ds(0, step)], mixed.at[:, pl.ds(0, step)], load_sems.at[7])
+    token_load = pltpu.make_async_copy(
+        tokens_hbm.at[:, pl.ds(step, (chunks - 1) * step)],
+        mixed.at[:, pl.ds(step, (chunks - 1) * step)],
+        load_sems.at[3],
+    )
     small_loads = [
         pltpu.make_async_copy(ids_hbm, route_ids, load_sems.at[4]),
         pltpu.make_async_copy(gates_hbm, route_gates, load_sems.at[5]),
         pltpu.make_async_copy(gain_hbm, gain, load_sems.at[6]),
     ]
+    first_load.start()
     token_load.start()
     for load in small_loads:
         load.start()
-    lax.fori_loop(0, half - 1, greet, 0)
+    lax.fori_loop(0, m - 1, greet, 0)
 
     @pl.when(is_hub)
     def _():
-        pl.semaphore_signal(barrier, inc=1, device_id={"ep": other_hub})
+        pl.semaphore_signal(barrier, inc=1, device_id={"ep": leaf + j})
 
     loads = [
         pltpu.make_async_copy(gate_hbm.at[0], w_gate, load_sems.at[0]),
         pltpu.make_async_copy(up_hbm.at[0], w_up, load_sems.at[1]),
         pltpu.make_async_copy(down_hbm.at[0], w_down, load_sems.at[2]),
     ]
-    token_load.wait()
+    first_load.wait()
 
     @pl.when(is_hub)
     def _():
-        pl.semaphore_wait(barrier, half)
+        pl.semaphore_wait(barrier, 1)
 
     @pl.when(jnp.logical_not(is_hub))
     def _():
@@ -273,12 +283,14 @@
             far_copy(ACROSS, c, raw(c), other_hub).start()
 
         across_out(0)
+        token_load.wait()
         build_table()
         table_copy(ACROSS, table, other_hub).start()
         each(1, lead, across_out)
         for load in loads:
             load.start()
         matrices(table, takes.at[HOME], gives.at[HOME], bases)
+        pl.semaphore_wait(ready, m)
         each(0, chunks, lambda c: pack(HOME, c, raw(c)))
         table_copy(NEAR, table, leaf + j).wait_recv()
         table_copy(BEYOND, tables.at[NEAR - 1], other_hub).start()
@@ -364,8 +376,9 @@
         def close(c):
             wait_back(HOME, c)
             relay_copy(HOME, c).wait_recv()
+            local[...] = dot32(gives[HOME], backs[HOME, c])
             part_copy(0, c, far.at[0], 0, other_hub).wait_recv()
-            finish(c, dot32(gives[HOME], backs[HOME, c]) + partial_in[0, c].astype(jnp.float32))
+            finish(c, local[...] + partial_in[0, c].astype(jnp.float32))
 
         each(0, chunks, close)
         for k in range(3):
@@ -374,6 +387,8 @@
     def leaf_role():
         lag = 2
         far_copy(NEAR, 0, raw(0), hub + j).start()
+        each(0, m, lambda i: pl.semaphore_signal(ready, inc=1, device_id={"ep": hub + (j + i) % m}))
+        token_load.wait()
         build_table()
         table_copy(NEAR, table, hub + j).start()
         each(1, chunks, lambda c: far_copy(NEAR, c, raw(c), hub + j).start())
@@ -463,7 +478,8 @@
             pltpu.VMEM((3, CHUNKS, 2 * unit, step), bf16),
             pltpu.VMEM((CHUNKS, unit, step), bf16),
             pltpu.VMEM((2, CHUNKS, rows, step), bf16),
-            dma((7,)),
+            pltpu.VMEM((rows, step), jnp.float32),
+            dma((8,)),
             dma((3,)),
             dma((3,)),
             dma((3,)),
@@ -476,6 +492,7 @@
             dma((3, CHUNKS)),
             dma((3,)),
             dma((2, CHUNKS)),
+            pltpu.SemaphoreType.REGULAR,
         ],
         compiler_params=pltpu.CompilerParams(
             collective_id=0, has_side_effects=True, vmem_limit_bytes=VMEM_BYTES

time: 188 us -> 186 us (0.989)
  no operation moved by 1% of the time
where the time goes in v5:
time: 186 us
  Pallas kernels  185 us (99%)
    pallas_call x1, Pallas kernels, body(): pl.pallas_call(functools.partial(kernel, devices, capacity, top), out_sha...  185 us

profile of v5, /device:TPU:15, one launch (start us, length us, event | category | flops | bytes accessed | tf_op | source)
XLA Modules:
  0.0 186.3 jit_solution(996984275542532468)
XLA Ops:
  0.0 184.9 %shard_map.73 = bf16[512,2048]{1,0:T(8,128)(2,1)S(1)} custom-call(bf16[512,2048]{1,0:T(8,128)(2,1)} %tokens_hbm.1, f32[1,2048]{1,0:T(1,128)} %bitcast.3, s32[2,512]{1,0:T(2,128)} %bitcast.4, f32[2,512]{1,0:T(2,128)} %bitcast.5, bf16[1,2048,1024]{2,1,0:T(8,128)(2,1)} %gate_hbm.1, bf16[1,2048,1024]{2,1,0:T(8,128)(2,1)} %up_hbm.1, bf16[1,1024,2048]{2,1,0:T(8,128)(2,1)} %down_hbm.1), custom_call_target="tpu_custom_call" | custom-call | tf_op jit(solution)/shard_map/pallas_call | solution.py:455
  184.9 1.3 copy.9

commit v6 on v5

--- a/solution.py
+++ b/solution.py
@@ -101,13 +101,24 @@
         return mixed.at[:, pl.ds(pl.multiple_of(c * step, step), step)]
 
     def table_copy(r, src, device):
-        return remote(src, tables.at[r - 1], table_send.at[r - 1], table_recv.at[r - 1], device)
-
-    def far_copy(r, c, src, device):
-        return remote(src, far.at[r - 1, c], far_send.at[r - 1], far_recv.at[r - 1, c], device)
-
-    def part_copy(k, c, src, slot, device):
-        return remote(src.at[c], partial_in.at[slot, c], part_send.at[k], part_recv.at[slot, c], device)
+        return remote(src, tables.at[r - 1], table_send, table_recv.at[r - 1], device)
+
+    def far_slot(r, c):
+        return far_recv.at[2 * chunks + c if r == ACROSS else (r - BEYOND) * chunks + c]
+
+    def far_copy(r, c, src, device, group=None):
+        send = far_send.at[1 if r == BEYOND else 0]
+        return remote(src, far.at[r - 1, c], send, far_slot(r, c if group is None else group), device)
+
+    def part_slot(slot, c):
+        return part_recv.at[chunks // 2 + 1 + c // 2 if slot else c // 2 + c // (chunks - 1)]
+
+    def part_copy(c, src, slot, device):
+        return remote(src.at[c], partial_in.at[slot, c], part_send, part_slot(slot, c), device)
+
+    def part_wait(slot, c, count):
+        got = partial_in.at[slot, pl.ds(c, count)]
+        remote(got, got, part_send, part_slot(slot, c), peer).wait_recv()
 
     def span(i, part=0):
         return pl.ds(pl.multiple_of(part * unit + i * capacity, 16), capacity)
@@ -122,32 +133,39 @@
         target = (leaf if part else own) + i
         return remote(
             packs(r, c).at[span(i, part)], arrived.at[r, c, span(j)],
-            go_send.at[r], go_recv.at[r], target,
+            go_send.at[r // NEAR], go_recv.at[r], target,
         )
 
     def settle(r, every):
         count = unit if every else unit - capacity
         got = arrived.at[r, :, pl.ds(0, count)]
-        remote(got, got, go_send.at[r], go_recv.at[r], peer).wait_recv()
-
-    def go_sent(r):
-        sent = packed_near.at[:, pl.ds(0, unit - capacity)] if r == NEAR else packed.at[r, :, pl.ds(0, 2 * unit - capacity)]
-        remote(sent, sent, go_send.at[r], go_recv.at[r], peer).wait_send()
+        remote(got, got, go_send.at[0], go_recv.at[r], peer).wait_recv()
+
+    def go_sent(near):
+        sent = packed_near.at[:, pl.ds(0, unit - capacity)] if near else packed.at[:, :, pl.ds(0, 2 * unit - capacity)]
+        remote(sent, sent, go_send.at[near], go_recv.at[0], peer).wait_send()
+
+    def back_slot(r, c):
+        if r == HOME:
+            return back_recv.at[c // 2]
+        if r == NEAR:
+            return back_recv.at[chunks // 2 + 2 * chunks]
+        return back_recv.at[chunks // 2 + (r - ACROSS) * chunks + c]
 
     def back_copy(r, c, i):
         return remote(
             arrived.at[r, c, span(i)], returns(r, c).at[span(j)],
-            back_send.at[r], back_recv.at[r, c], own + i,
+            back_send, back_slot(r, c), own + i,
         )
 
-    def back_sent(r):
-        sent = arrived.at[r, :, pl.ds(0, unit - capacity)]
-        remote(sent, sent, back_send.at[r], go_recv.at[r], peer).wait_send()
+    def back_sent():
+        sent = arrived.at[:, :, pl.ds(0, unit - capacity)]
+        remote(sent, sent, back_send, go_recv.at[0], peer).wait_send()
 
     def relay_copy(r, c):
         return remote(
             backs.at[r, c, pl.ds(0, unit)], backs.at[r, c, pl.ds(unit, unit)],
-            relay_send.at[r], relay_recv.at[r, c], hub + j,
+            relay_send, relay_recv.at[0 if r == HOME else 1 + (r - ACROSS) * chunks + c], hub + j,
         )
 
     def others(act):
@@ -269,7 +287,15 @@
 
     def wait_back(r, c):
         got = returns(r, c).at[pl.ds(0, unit - capacity)]
-        remote(got, got, back_send.at[r], back_recv.at[r, c], peer).wait_recv()
+        remote(got, got, back_send, back_slot(r, c), peer).wait_recv()
+
+    def wait_home(p):
+        got = backs.at[HOME, pl.ds(2 * p, 2), pl.ds(0, unit - capacity)]
+        remote(got, got, back_send, back_slot(HOME, 2 * p), peer).wait_recv()
+
+    def wait_near():
+        got = backs_near.at[:, pl.ds(0, unit - capacity)]
+        remote(got, got, back_send, back_slot(NEAR, 0), peer).wait_recv()
 
     def all_sent(sem, ref):
         remote(ref, ref, sem, go_recv.at[0], peer).wait_send()
@@ -279,14 +305,14 @@
         lead = 2
         mid = chunks // 2
 
-        def across_out(c):
-            far_copy(ACROSS, c, raw(c), other_hub).start()
-
-        across_out(0)
+        def across_out(c, group):
+            far_copy(ACROSS, c, raw(c), other_hub, group).start()
+
+        across_out(0, 0)
         token_load.wait()
         build_table()
         table_copy(ACROSS, table, other_hub).start()
-        each(1, lead, across_out)
+        each(1, lead, lambda c: across_out(c, 0))
         for load in loads:
             load.start()
         matrices(table, takes.at[HOME], gives.at[HOME], bases)
@@ -309,21 +335,28 @@
             wait_back(r, c)
             relay_copy(r, c).wait_recv()
             far[r - 1, c] = dot32(gives[r], backs[r, c]).astype(jnp.bfloat16)
-            slot = 0 if r == ACROSS else 1
-            part_copy(slot, c, far.at[r - 1], slot, other_hub).start()
-
-        def pass_on(c):
-            wait_back(NEAR, c)
-            part_copy(1, c, far.at[0], 1, other_hub).wait_recv()
-            total = dot32(give_near[...], backs_near[c]) + partial_in[1, c].astype(jnp.float32)
-            far[NEAR - 1, c] = total.astype(jnp.bfloat16)
-            part_copy(2, c, far.at[NEAR - 1], 1, leaf + j).start()
+            part_copy(c, far.at[r - 1], 0 if r == ACROSS else 1, other_hub).start()
+
+        def pass_on(p):
+            part_wait(1, 2 * p, 2)
+
+            def one(c):
+                total = dot32(give_near[...], backs_near[c]) + partial_in[1, c].astype(jnp.float32)
+                far[NEAR - 1, c] = total.astype(jnp.bfloat16)
+                part_copy(c, far.at[NEAR - 1], 1, leaf + j).start()
+
+            each(2 * p, 2 * p + 2, one)
 
         def beyond_in(c):
             far_in(BEYOND, c)
 
-        def across_in(c):
-            far_in(ACROSS, c)
+        def across_in(low, count, group):
+            got = far.at[ACROSS - 1, pl.ds(low, count)]
+            remote(got, got, far_send.at[0], far_slot(ACROSS, group), peer).wait_recv()
+            each(low, low + count, lambda c: pack(ACROSS, c, far.at[ACROSS - 1, c]))
+
+        def across_one(c):
+            across_in(c, 1, c - mid + 1)
 
         each(0, lead, near_in)
         table_copy(ACROSS, table, other_hub).wait_recv()
@@ -336,56 +369,61 @@
             near_in(c + lead)
 
         each(0, chunks - lead, early)
-        each(lead, chunks, across_out)
+        each(lead, mid + 1, lambda c: across_out(c, 1))
+        each(mid + 1, chunks, lambda c: across_out(c, c - mid + 1))
         for load in loads:
             load.wait()
         settle(HOME, False)
         expert(HOME, False)
         each(chunks - lead, chunks, beyond_in)
-        each(0, lead, across_in)
+        across_in(0, lead, 0)
         settle(NEAR, False)
         expert(NEAR, False)
         settle(BEYOND, False)
         expert(BEYOND, True)
-        each(lead, mid + 1, across_in)
-        each(mid + 1, chunks - 1, across_in)
+        across_in(lead, mid + 1 - lead, 1)
+        each(mid + 1, chunks - 1, across_one)
         merge(BEYOND, 0)
-        across_in(chunks - 1)
+        across_one(chunks - 1)
         each(0, chunks, lambda c: hand_back(NEAR, c))
         each(1, mid + lead, lambda c: merge(BEYOND, c))
-        all_sent(far_send.at[BEYOND - 1], far.at[NEAR - 1])
+        all_sent(far_send.at[1], far.at[NEAR - 1])
         settle(ACROSS, False)
         expert(ACROSS, True)
         each(mid + lead, chunks, lambda c: merge(BEYOND, c))
         each(0, chunks, lambda c: hand_back(HOME, c))
-        each(0, mid, pass_on)
-
-        def late(c):
-            pass_on(c)
-            merge(ACROSS, c - mid)
-
-        each(mid, chunks, late)
+        wait_near()
+        each(0, mid // 2, pass_on)
+
+        def late(p):
+            pass_on(p)
+            each(2 * p - mid, 2 * p - mid + 2, lambda c: merge(ACROSS, c))
+
+        each(mid // 2, chunks // 2, late)
         each(mid, chunks, lambda c: merge(ACROSS, c))
-        all_sent(table_send.at[ACROSS - 1], table)
-        all_sent(table_send.at[BEYOND - 1], table)
-        all_sent(far_send.at[ACROSS - 1], mixed)
-        for r in range(4):
-            go_sent(r)
-            back_sent(r)
-
-        def close(c):
-            wait_back(HOME, c)
-            relay_copy(HOME, c).wait_recv()
+        all_sent(table_send, tables.at[pl.ds(0, 2)])
+        all_sent(far_send.at[0], mixed)
+        go_sent(0)
+        go_sent(1)
+        back_sent()
+        each(0, chunks // 2, wait_home)
+        got = backs.at[HOME, :, pl.ds(0, unit)]
+        remote(got, got, relay_send, relay_recv.at[0], peer).wait_recv()
+
+        def close(c, wait):
             local[...] = dot32(gives[HOME], backs[HOME, c])
-            part_copy(0, c, far.at[0], 0, other_hub).wait_recv()
+            wait()
             finish(c, local[...] + partial_in[0, c].astype(jnp.float32))
 
-        each(0, chunks, close)
-        for k in range(3):
-            all_sent(part_send.at[k], far.at[0])
+        def close_pair(p):
+            close(2 * p, lambda: part_wait(0, 2 * p, 2))
+            close(2 * p + 1, lambda: None)
+
+        each(0, chunks // 2 - 1, close_pair)
+        each(chunks - 2, chunks, lambda c: close(c, lambda: part_wait(0, c, 1)))
+        all_sent(part_send, far)
 
     def leaf_role():
-        lag = 2
         far_copy(NEAR, 0, raw(0), hub + j).start()
         each(0, m, lambda i: pl.semaphore_signal(ready, inc=1, device_id={"ep": hub + (j + i) % m}))
         token_load.wait()
@@ -402,33 +440,37 @@
             wait_back(r, c)
             relay_copy(r, c).start()
 
+        def send_home(p):
+            wait_home(p)
+            each(2 * p, 2 * p + 2, lambda c: relay_copy(HOME, c).start())
+
         settle(HOME, True)
         expert(HOME, True)
-        each(0, chunks - lag, lambda c: send_on(HOME, c))
+        each(0, chunks // 2 - 1, send_home)
         settle(BEYOND, True)
         expert(BEYOND, True)
         each(0, chunks, lambda c: send_on(BEYOND, c))
-        each(chunks - lag, chunks, lambda c: send_on(HOME, c))
+        send_home(chunks // 2 - 1)
         settle(ACROSS, True)
         expert(ACROSS, True)
         each(0, chunks, lambda c: pack(NEAR, c, raw(c)))
         each(0, chunks, lambda c: send_on(ACROSS, c))
         settle(NEAR, False)
         expert(NEAR, True)
-        all_sent(table_send.at[NEAR - 1], table)
-        all_sent(far_send.at[NEAR - 1], mixed)
-
-        def close(c):
-            wait_back(NEAR, c)
-            part_copy(2, c, far.at[0], 1, hub + j).wait_recv()
-            finish(c, dot32(give_near[...], backs_near[c]) + partial_in[1, c].astype(jnp.float32))
-
-        each(0, chunks, close)
-        go_sent(NEAR)
-        for r in range(4):
-            back_sent(r)
-        for r in (HOME, ACROSS, BEYOND):
-            all_sent(relay_send.at[r], backs.at[r, :, pl.ds(0, unit)])
+        all_sent(table_send, table)
+        all_sent(far_send.at[0], mixed)
+
+        wait_near()
+
+        def close_pair(p):
+            part_wait(1, 2 * p, 2)
+            for c in (2 * p, 2 * p + 1):
+                finish(c, dot32(give_near[...], backs_near[c]) + partial_in[1, c].astype(jnp.float32))
+
+        each(0, chunks // 2, close_pair)
+        go_sent(1)
+        back_sent()
+        all_sent(relay_send, backs.at[:, :, pl.ds(0, unit)])
 
     @pl.when(is_hub)
     def _():
@@ -480,18 +522,18 @@
             pltpu.VMEM((2, CHUNKS, rows, step), bf16),
             pltpu.VMEM((rows, step), jnp.float32),
             dma((8,)),
+            dma,
             dma((3,)),
-            dma((3,)),
-            dma((3,)),
-            dma((3, CHUNKS)),
+            dma((2,)),
+            dma((2 * CHUNKS + CHUNKS // 2 + 1,)),
+            dma((2,)),
             dma((4,)),
-            dma((4,)),
-            dma((4,)),
-            dma((4, CHUNKS)),
-            dma((3,)),
-            dma((3, CHUNKS)),
-            dma((3,)),
-            dma((2, CHUNKS)),
+            dma,
+            dma((CHUNKS // 2 + 2 * CHUNKS + 1,)),
+            dma,
+            dma((1 + 2 * CHUNKS,)),
+            dma,
+            dma((CHUNKS // 2 + 1 + CHUNKS // 2,)),
             pltpu.SemaphoreType.REGULAR,
         ],
         compiler_params=pltpu.CompilerParams(

time: 186 us -> 186 us (level)
  no operation moved by 1% of the time
where the time goes in v6:
time: 186 us
  Pallas kernels  185 us (99%)
    pallas_call x1, Pallas kernels, body(): pl.pallas_call(functools.partial(kernel, devices, capacity, top), out_sha...  185 us

profile of v6, /device:TPU:15, one launch (start us, length us, event | category | flops | bytes accessed | tf_op | source)
XLA Modules:
  0.0 185.9 jit_solution(10123319021914176319)
XLA Ops:
  0.0 184.6 %shard_map.73 = bf16[512,2048]{1,0:T(8,128)(2,1)S(1)} custom-call(bf16[512,2048]{1,0:T(8,128)(2,1)} %tokens_hbm.1, f32[1,2048]{1,0:T(1,128)} %bitcast.3, s32[2,512]{1,0:T(2,128)} %bitcast.4, f32[2,512]{1,0:T(2,128)} %bitcast.5, bf16[1,2048,1024]{2,1,0:T(8,128)(2,1)} %gate_hbm.1, bf16[1,2048,1024]{2,1,0:T(8,128)(2,1)} %up_hbm.1, bf16[1,1024,2048]{2,1,0:T(8,128)(2,1)} %down_hbm.1), custom_call_target="tpu_custom_call" | custom-call | tf_op jit(solution)/shard_map/pallas_call | solution.py:497
  184.6 1.3 copy.9

commit v7 on v6

--- a/solution.py
+++ b/solution.py
@@ -27,7 +27,7 @@
     gain, route_ids, route_gates, table, far, tables, takes, gives, take_near, give_near, packed, packed_near, arrived, hidden,
     w_gate, w_up, w_down, backs, backs_near, partial_in, local,
     load_sems, table_send, table_recv, far_send, far_recv, go_send, go_recv, back_send, back_recv,
-    relay_send, relay_recv, part_send, part_recv, ready,
+    home_recv, part_send, part_recv, ready,
 ):
     m = devices // 4
     half = 2 * m
@@ -111,7 +111,7 @@
         return remote(src, far.at[r - 1, c], send, far_slot(r, c if group is None else group), device)
 
     def part_slot(slot, c):
-        return part_recv.at[chunks // 2 + 1 + c // 2 if slot else c // 2 + c // (chunks - 1)]
+        return part_recv.at[c // 2] if slot else far_slot(ACROSS, c // 2 + c // (chunks - 1))
 
     def part_copy(c, src, slot, device):
         return remote(src.at[c], partial_in.at[slot, c], part_send, part_slot(slot, c), device)
@@ -146,11 +146,11 @@
         remote(sent, sent, go_send.at[near], go_recv.at[0], peer).wait_send()
 
     def back_slot(r, c):
-        if r == HOME:
-            return back_recv.at[c // 2]
+        if r == BEYOND:
+            return back_recv.at[c]
         if r == NEAR:
-            return back_recv.at[chunks // 2 + 2 * chunks]
-        return back_recv.at[chunks // 2 + (r - ACROSS) * chunks + c]
+            return back_recv.at[2 * chunks]
+        return back_recv.at[chunks + (0 if r == HOME else chunks // 2) + c // 2]
 
     def back_copy(r, c, i):
         return remote(
@@ -162,10 +162,15 @@
         sent = arrived.at[:, :, pl.ds(0, unit - capacity)]
         remote(sent, sent, back_send, go_recv.at[0], peer).wait_send()
 
+    def relay_slot(r, c):
+        if r == HOME:
+            return home_recv
+        return far_slot(NEAR if r == BEYOND else BEYOND, c)
+
     def relay_copy(r, c):
         return remote(
             backs.at[r, c, pl.ds(0, unit)], backs.at[r, c, pl.ds(unit, unit)],
-            relay_send, relay_recv.at[0 if r == HOME else 1 + (r - ACROSS) * chunks + c], hub + j,
+            part_send, relay_slot(r, c), hub + j,
         )
 
     def others(act):
@@ -289,9 +294,9 @@
         got = returns(r, c).at[pl.ds(0, unit - capacity)]
         remote(got, got, back_send, back_slot(r, c), peer).wait_recv()
 
-    def wait_home(p):
-        got = backs.at[HOME, pl.ds(2 * p, 2), pl.ds(0, unit - capacity)]
-        remote(got, got, back_send, back_slot(HOME, 2 * p), peer).wait_recv()
+    def wait_pair(r, p):
+        got = backs.at[r, pl.ds(2 * p, 2), pl.ds(0, unit - capacity)]
+        remote(got, got, back_send, back_slot(r, 2 * p), peer).wait_recv()
 
     def wait_near():
         got = backs_near.at[:, pl.ds(0, unit - capacity)]
@@ -332,10 +337,15 @@
             pack(r, c, far.at[r - 1, c])
 
         def merge(r, c):
-            wait_back(r, c)
+            if r == BEYOND:
+                wait_back(r, c)
             relay_copy(r, c).wait_recv()
             far[r - 1, c] = dot32(gives[r], backs[r, c]).astype(jnp.bfloat16)
             part_copy(c, far.at[r - 1], 0 if r == ACROSS else 1, other_hub).start()
+
+        def merge_pair(p):
+            wait_pair(ACROSS, p)
+            each(2 * p, 2 * p + 2, lambda c: merge(ACROSS, c))
 
         def pass_on(p):
             part_wait(1, 2 * p, 2)
@@ -397,18 +407,18 @@
 
         def late(p):
             pass_on(p)
-            each(2 * p - mid, 2 * p - mid + 2, lambda c: merge(ACROSS, c))
+            merge_pair(p - mid // 2)
 
         each(mid // 2, chunks // 2, late)
-        each(mid, chunks, lambda c: merge(ACROSS, c))
+        each(mid // 2, chunks // 2, merge_pair)
         all_sent(table_send, tables.at[pl.ds(0, 2)])
         all_sent(far_send.at[0], mixed)
         go_sent(0)
         go_sent(1)
         back_sent()
-        each(0, chunks // 2, wait_home)
+        each(0, chunks // 2, lambda p: wait_pair(HOME, p))
         got = backs.at[HOME, :, pl.ds(0, unit)]
-        remote(got, got, relay_send, relay_recv.at[0], peer).wait_recv()
+        remote(got, got, part_send, home_recv, peer).wait_recv()
 
         def close(c, wait):
             local[...] = dot32(gives[HOME], backs[HOME, c])
@@ -436,25 +446,25 @@
         for load in loads:
             load.wait()
 
-        def send_on(r, c):
-            wait_back(r, c)
-            relay_copy(r, c).start()
-
-        def send_home(p):
-            wait_home(p)
-            each(2 * p, 2 * p + 2, lambda c: relay_copy(HOME, c).start())
+        def send_on(c):
+            wait_back(BEYOND, c)
+            relay_copy(BEYOND, c).start()
+
+        def send_pair(r, p):
+            wait_pair(r, p)
+            each(2 * p, 2 * p + 2, lambda c: relay_copy(r, c).start())
 
         settle(HOME, True)
         expert(HOME, True)
-        each(0, chunks // 2 - 1, send_home)
+        each(0, chunks // 2 - 1, lambda p: send_pair(HOME, p))
         settle(BEYOND, True)
         expert(BEYOND, True)
-        each(0, chunks, lambda c: send_on(BEYOND, c))
-        send_home(chunks // 2 - 1)
+        each(0, chunks, send_on)
+        send_pair(HOME, chunks // 2 - 1)
         settle(ACROSS, True)
         expert(ACROSS, True)
         each(0, chunks, lambda c: pack(NEAR, c, raw(c)))
-        each(0, chunks, lambda c: send_on(ACROSS, c))
+        each(0, chunks // 2, lambda p: send_pair(ACROSS, p))
         settle(NEAR, False)
         expert(NEAR, True)
         all_sent(table_send, table)
@@ -470,7 +480,7 @@
         each(0, chunks // 2, close_pair)
         go_sent(1)
         back_sent()
-        all_sent(relay_send, backs.at[:, :, pl.ds(0, unit)])
+        all_sent(part_send, backs.at[:, :, pl.ds(0, unit)])
 
     @pl.when(is_hub)
     def _():
@@ -529,11 +539,10 @@
             dma((2,)),
             dma((4,)),
             dma,
-            dma((CHUNKS // 2 + 2 * CHUNKS + 1,)),
+            dma((2 * CHUNKS + 1,)),
             dma,
-            dma((1 + 2 * CHUNKS,)),
             dma,
-            dma((CHUNKS // 2 + 1 + CHUNKS // 2,)),
+            dma((CHUNKS // 2,)),
             pltpu.SemaphoreType.REGULAR,
         ],
         compiler_params=pltpu.CompilerParams(

time: 186 us -> 186 us (level)
  no operation moved by 1% of the time
where the time goes in v7:
time: 186 us
  Pallas kernels  184 us (99%)
    pallas_call x1, Pallas kernels, body(): pl.pallas_call(functools.partial(kernel, devices, capacity, top), out_sha...  184 us

profile of v7, /device:TPU:15, one launch (start us, length us, event | category | flops | bytes accessed | tf_op | source)
XLA Modules:
  0.0 185.7 jit_solution(6140478936065963674)
XLA Ops:
  0.0 184.3 %shard_map.73 = bf16[512,2048]{1,0:T(8,128)(2,1)S(1)} custom-call(bf16[512,2048]{1,0:T(8,128)(2,1)} %tokens_hbm.1, f32[1,2048]{1,0:T(1,128)} %bitcast.3, s32[2,512]{1,0:T(2,128)} %bitcast.4, f32[2,512]{1,0:T(2,128)} %bitcast.5, bf16[1,2048,1024]{2,1,0:T(8,128)(2,1)} %gate_hbm.1, bf16[1,2048,1024]{2,1,0:T(8,128)(2,1)} %up_hbm.1, bf16[1,1024,2048]{2,1,0:T(8,128)(2,1)} %down_hbm.1), custom_call_target="tpu_custom_call" | custom-call | tf_op jit(solution)/shard_map/pallas_call | solution.py:507
  184.3 1.3 copy.9

commit v8 on v7

--- a/solution.py
+++ b/solution.py
@@ -26,7 +26,7 @@
     mixed,
     gain, route_ids, route_gates, table, far, tables, takes, gives, take_near, give_near, packed, packed_near, arrived, hidden,
     w_gate, w_up, w_down, backs, backs_near, partial_in, local,
-    load_sems, table_send, table_recv, far_send, far_recv, go_send, go_recv, back_send, back_recv,
+    load_sems, table_send, far_send, far_recv, go_send, go_recv, back_send, back_recv,
     home_recv, part_send, part_recv, ready,
 ):
     m = devices // 4
@@ -56,16 +56,16 @@
         pl.semaphore_signal(barrier, inc=1, device_id={"ep": leaf + (j + 1 + i) % m})
         return carry
 
-    first_load = pltpu.make_async_copy(tokens_hbm.at[:, pl.ds(0, step)], mixed.at[:, pl.ds(0, step)], load_sems.at[7])
+    first_load = pltpu.make_async_copy(tokens_hbm.at[:, pl.ds(0, step)], mixed.at[:, pl.ds(0, step)], load_sems.at[4])
     token_load = pltpu.make_async_copy(
         tokens_hbm.at[:, pl.ds(step, (chunks - 1) * step)],
         mixed.at[:, pl.ds(step, (chunks - 1) * step)],
-        load_sems.at[3],
+        load_sems.at[0],
     )
     small_loads = [
-        pltpu.make_async_copy(ids_hbm, route_ids, load_sems.at[4]),
-        pltpu.make_async_copy(gates_hbm, route_gates, load_sems.at[5]),
-        pltpu.make_async_copy(gain_hbm, gain, load_sems.at[6]),
+        pltpu.make_async_copy(ids_hbm, route_ids, load_sems.at[1]),
+        pltpu.make_async_copy(gates_hbm, route_gates, load_sems.at[2]),
+        pltpu.make_async_copy(gain_hbm, gain, load_sems.at[3]),
     ]
     first_load.start()
     token_load.start()
@@ -78,9 +78,9 @@
         pl.semaphore_signal(barrier, inc=1, device_id={"ep": leaf + j})
 
     loads = [
-        pltpu.make_async_copy(gate_hbm.at[0], w_gate, load_sems.at[0]),
-        pltpu.make_async_copy(up_hbm.at[0], w_up, load_sems.at[1]),
-        pltpu.make_async_copy(down_hbm.at[0], w_down, load_sems.at[2]),
+        pltpu.make_async_copy(gate_hbm.at[0], w_gate, part_recv.at[0]),
+        pltpu.make_async_copy(up_hbm.at[0], w_up, part_recv.at[1]),
+        pltpu.make_async_copy(down_hbm.at[0], w_down, part_recv.at[2]),
     ]
     first_load.wait()
 
@@ -101,7 +101,7 @@
         return mixed.at[:, pl.ds(pl.multiple_of(c * step, step), step)]
 
     def table_copy(r, src, device):
-        return remote(src, tables.at[r - 1], table_send, table_recv.at[r - 1], device)
+        return remote(src, tables.at[r - 1], table_send, load_sems.at[5 + r - 1], device)
 
     def far_slot(r, c):
         return far_recv.at[2 * chunks + c if r == ACROSS else (r - BEYOND) * chunks + c]
@@ -147,10 +147,10 @@
 
     def back_slot(r, c):
         if r == BEYOND:
-            return back_recv.at[c]
+            return load_sems.at[c]
         if r == NEAR:
-            return back_recv.at[2 * chunks]
-        return back_recv.at[chunks + (0 if r == HOME else chunks // 2) + c // 2]
+            return back_recv.at[chunks]
+        return back_recv.at[(0 if r == HOME else chunks // 2) + c // 2]
 
     def back_copy(r, c, i):
         return remote(
@@ -378,11 +378,11 @@
             beyond_in(c)
             near_in(c + lead)
 
+        for load in loads:
+            load.wait()
         each(0, chunks - lead, early)
         each(lead, mid + 1, lambda c: across_out(c, 1))
         each(mid + 1, chunks, lambda c: across_out(c, c - mid + 1))
-        for load in loads:
-            load.wait()
         settle(HOME, False)
         expert(HOME, False)
         each(chunks - lead, chunks, beyond_in)
@@ -531,15 +531,14 @@
             pltpu.VMEM((CHUNKS, unit, step), bf16),
             pltpu.VMEM((2, CHUNKS, rows, step), bf16),
             pltpu.VMEM((rows, step), jnp.float32),
-            dma((8,)),
+            dma((max(8, CHUNKS),)),
             dma,
-            dma((3,)),
             dma((2,)),
             dma((2 * CHUNKS + CHUNKS // 2 + 1,)),
             dma((2,)),
             dma((4,)),
             dma,
-            dma((2 * CHUNKS + 1,)),
+            dma((CHUNKS + 1,)),
             dma,
             dma,
             dma((CHUNKS // 2,)),

time: 186 us -> 186 us (level)
  no operation moved by 1% of the time
where the time goes in v8:
time: 186 us
  Pallas kernels  184 us (99%)
    pallas_call x1, Pallas kernels, body(): pl.pallas_call(functools.partial(kernel, devices, capacity, top), out_sha...  184 us

profile of v8, /device:TPU:15, one launch (start us, length us, event | category | flops | bytes accessed | tf_op | source)
XLA Modules:
  0.0 185.6 jit_solution(6855984223578356165)
XLA Ops:
  0.0 184.2 %shard_map.73 = bf16[512,2048]{1,0:T(8,128)(2,1)S(1)} custom-call(bf16[512,2048]{1,0:T(8,128)(2,1)} %tokens_hbm.1, f32[1,2048]{1,0:T(1,128)} %bitcast.3, s32[2,512]{1,0:T(2,128)} %bitcast.4, f32[2,512]{1,0:T(2,128)} %bitcast.5, bf16[1,2048,1024]{2,1,0:T(8,128)(2,1)} %gate_hbm.1, bf16[1,2048,1024]{2,1,0:T(8,128)(2,1)} %up_hbm.1, bf16[1,1024,2048]{2,1,0:T(8,128)(2,1)} %down_hbm.1), custom_call_target="tpu_custom_call" | custom-call | tf_op jit(solution)/shard_map/pallas_call | solution.py:507
  184.2 1.3 copy.9
